TPU v7x, 32 devices: a whole 2x2x4 slice. The times are simulated.
32 devices in a mesh: kv: 8 (over z, x), tp: 4 (over y, core).
Axes of the slice: x: 2, y: 2, z: 4, core: 2. Of those that a mesh axis runs over, the one named last changes fastest.
Arguments:
- tokens: bfloat16 [64, 12, 4096], P(None, None, 'kv'), may hold values from -6 to 6
- parents: int32 [64, 12], P('kv'), may hold values from -1 to 10, as said below
- accepted: int32 [64], P('kv'), may hold values from 0 to 6
- state: float32 [64, 64, 64, 128], P('kv', 'tp'), may hold values from -4 to 4
- conv_x: bfloat16 [64, 3, 4096], P('kv', None, 'tp'), may hold values from -6 to 6
- conv_b: bfloat16 [64, 3, 2048], P('kv', None, 'tp'), may hold values from -6 to 6
- conv_c: bfloat16 [64, 3, 2048], P('kv', None, 'tp'), may hold values from -6 to 6
- path_x: bfloat16 [64, 6, 4096], P('kv', None, 'tp'), may hold values from -6 to 6
- path_b: bfloat16 [64, 6, 2048], P('kv', None, 'tp'), may hold values from -6 to 6
- path_c: bfloat16 [64, 6, 2048], P('kv', None, 'tp'), may hold values from -6 to 6
- path_dt: bfloat16 [64, 6, 64], P('kv', None, 'tp'), may hold values from -6 to 6
- gain_in: float32 [4096], replicated, may hold values from 0.1 to 1.9
- w_x: bfloat16 [4096, 4096], P('kv', 'tp'), may hold values from -0.09375 to 0.09375
- w_z: bfloat16 [4096, 4096], P('kv', 'tp'), may hold values from -0.09375 to 0.09375
- w_b: bfloat16 [4096, 2048], P('kv', 'tp'), may hold values from -0.09375 to 0.09375
- w_c: bfloat16 [4096, 2048], P('kv', 'tp'), may hold values from -0.09375 to 0.09375
- w_dt: bfloat16 [4096, 64], replicated, may hold values from -0.09375 to 0.09375
- dt_bias: float32 [64], P('tp'), may hold values from -2 to 1
- a_log: float32 [64], P('tp'), may hold values from -3 to 1.5
- d_skip: float32 [64], P('tp'), may hold values from 0.5 to 1.5
- conv_wx: bfloat16 [4, 4096], P(None, 'tp'), may hold values from -3 to 3
- conv_wb: bfloat16 [4, 2048], P(None, 'tp'), may hold values from -3 to 3
- conv_wc: bfloat16 [4, 2048], P(None, 'tp'), may hold values from -3 to 3
- gain_out: float32 [4096], P('tp'), may hold values from 0.1 to 1.9
- w_out: bfloat16 [4096, 4096], P('tp', 'kv'), may hold values from -0.09375 to 0.09375
Outputs:
- mixed: bfloat16 [64, 12, 4096], P('kv', None, 'tp')
- new_state: float32 [64, 64, 64, 128], P('kv', 'tp')
Inputs may be any that keep to these rules, and one draw needn't show every extreme that they name: `parents`: each proposal's parent is -1 or an earlier proposal of the same sequence; the first proposal's parent is -1.
All inputs are finite; a program needn't handle non-finite values.
Results may differ from a plain program's by a relative error of at most 0.03.
Values may be sent and summed in bfloat16 or wider, within the bound.
No kernel may reach another device: no remote copies, remote signals or barrier semaphores. Data moves between devices by JAX's collectives and lax.ppermute only.
A program may use at most 128 MiB of HBM per device.

v0:
```python
import functools

import jax
import jax.numpy as jnp
from jax import lax
from jax.experimental import pallas as pl
from jax.experimental.pallas import tpu as pltpu
from jax.sharding import PartitionSpec as P


HPG = 4
EPS = 1e-06
LANES = 128
CHUNK = 256
VMEM = pltpu.VMEM
F32 = jnp.float32
BF16 = jnp.bfloat16
NT = (((1,), (1,)), ((), ()))


def log2(count):
    return count.bit_length() - 1


def flipped_bits(position, order):
    value = 0
    for place, bit in enumerate(order):
        value |= ((position >> (len(order) - 1 - place)) & 1) << bit
    return value


def whole(count):
    return [pl.BlockSpec(memory_space=VMEM) for _ in range(count)]


def cost(microseconds):
    return pl.CostEstimate(
        flops=int(microseconds * 4e6), bytes_accessed=1024, transcendentals=0
    )


def dot(left, right):
    return jnp.dot(left, right, preferred_element_type=F32)


def dot_nt(left, right):
    return lax.dot_general(left, right, NT, preferred_element_type=F32)


def silu(values):
    return values / (1.0 + jnp.exp(-values))


def softplus(values):
    return jnp.maximum(values, 0.0) + jnp.log1p(jnp.exp(-jnp.abs(values)))


def project_kernel(differences, with_rate, tp_count, tokens_ref, gain_ref, *refs):
    props, _, seqs, width = tokens_ref.shape
    me = lax.axis_index("kv")
    rows_local = props * seqs
    if with_rate:
        w_dt_ref, *w_refs, out_ref, scaled_ref, squares_ref = refs
    else:
        *w_refs, out_ref, scaled_ref = refs
    slab_start = pl.multiple_of(me * width, LANES)
    gain = gain_ref[:, pl.ds(slab_start, width)]
    for position, difference in enumerate(differences):
        rows = tokens_ref[:, me ^ difference].astype(F32).reshape(rows_local, width)
        span = slice(position * rows_local, (position + 1) * rows_local)
        scaled_ref[span] = (rows * gain).astype(BF16)
        if with_rate:
            squares_ref[span] = jnp.sum(rows * rows, axis=1, keepdims=True)
    start = 0
    for w_ref in w_refs:
        for lower in range(0, w_ref.shape[1], CHUNK):
            upper = min(lower + CHUNK, w_ref.shape[1])
            out_ref[:, start + lower : start + upper] = dot(
                scaled_ref[...], w_ref[:, lower:upper]
            ).astype(BF16)
        start += w_ref.shape[1]
    if with_rate:
        heads = w_dt_ref.shape[0]
        local = heads // tp_count
        first = lax.axis_index("tp") * local
        row = lax.broadcasted_iota(jnp.int32, (LANES, heads), 0)
        column = lax.broadcasted_iota(jnp.int32, (LANES, heads), 1)
        pick = jnp.where((row < local) & (column == row + first), 1.0, 0.0).astype(BF16)
        slab = w_dt_ref[:, pl.ds(slab_start, width)]
        w_rate = dot(pick, slab).astype(BF16)
        lane = lax.broadcasted_iota(jnp.int32, (1, LANES), 1)
        rate = dot_nt(scaled_ref[...], w_rate)
        out_ref[:, start : start + LANES] = jnp.where(
            lane == local, squares_ref[...], rate
        ).astype(BF16)


def project(differences, tokens, tp_count, gain, weights, w_dt=None):
    props, _, seqs, width = tokens.shape
    rows = len(differences) * props * seqs
    columns = sum(weight.shape[1] for weight in weights)
    scratch = [pltpu.VMEM((rows, width), BF16)]
    operands = [tokens, gain]
    if w_dt is not None:
        columns += LANES
        scratch.append(pltpu.VMEM((rows, 1), F32))
        operands.append(w_dt)
    operands += list(weights)
    return pl.pallas_call(
        functools.partial(project_kernel, tuple(differences), w_dt is not None, tp_count),
        out_shape=jax.ShapeDtypeStruct((rows, columns), BF16),
        in_specs=whole(len(operands)),
        out_specs=pl.BlockSpec(memory_space=VMEM),
        scratch_shapes=scratch,
        cost_estimate=cost(2),
        name="project",
    )(*operands)


def window(conv_ref, path_ref, taps_ref, seqs):
    history = jnp.concatenate([conv_ref[...].astype(F32), path_ref[...].astype(F32)], axis=0)
    count = path_ref.shape[0]
    taps = taps_ref[...].astype(F32)
    total = taps[0:1] * history[0:count]
    for distance in range(1, taps.shape[0]):
        total = total + taps[distance : distance + 1] * history[
            distance * seqs : distance * seqs + count
        ]
    return silu(total)


def split(values):
    high = values.astype(BF16).astype(F32)
    return high, values - high


def state_kernel(
    accepted_ref,
    path_dt_ref,
    bias_ref,
    a_log_ref,
    conv_x_ref,
    path_x_ref,
    taps_x_ref,
    conv_b_ref,
    path_b_ref,
    taps_b_ref,
    state_ref,
    out_ref,
    half_ref,
    left_ref,
    right_ref,
    decay_ref,
):
    _, heads, head_dim, state_dim = state_ref.shape
    seqs = accepted_ref.shape[0]
    sequence = pl.program_id(0)
    count = path_x_ref.shape[0]
    group_width = HPG * head_dim

    @pl.when(sequence == 0)
    def _():
        lane = lax.broadcasted_iota(jnp.int32, (heads, heads * head_dim), 1)
        row = lax.broadcasted_iota(jnp.int32, (heads, heads * head_dim), 0)
        spread = jnp.where(lane // head_dim == row, 1.0, 0.0).astype(BF16)
        accepted = accepted_ref[...]
        a_rate = -jnp.exp(a_log_ref[...])
        steps = softplus(path_dt_ref[...].astype(F32) + bias_ref[...])
        weights = []
        overall = jnp.zeros((seqs, heads), F32)
        for position in range(count // seqs - 1, -1, -1):
            step = steps[position * seqs : (position + 1) * seqs]
            live = jnp.where(position < accepted, 1.0, 0.0)
            weights.append(live * jnp.exp(overall) * step)
            overall = overall + step * a_rate * live
        decay_ref[...] = jnp.exp(overall)
        high, low = split(jnp.concatenate(weights[::-1], axis=0))
        weights = dot(high.astype(BF16), spread) + dot(low.astype(BF16), spread)
        grown = weights * window(conv_x_ref, path_x_ref, taps_x_ref, seqs)
        empty = jnp.zeros((LANES - 2 * count, grown.shape[1]), F32)
        turned = jnp.concatenate([grown, grown, empty], axis=0).T
        high, low = split(turned)
        left_ref[:, :LANES] = high.astype(BF16)
        left_ref[:, LANES:] = low.astype(BF16)
        rows_b = window(conv_b_ref, path_b_ref, taps_b_ref, seqs)
        high, low = split(rows_b)
        right_ref[...] = jnp.zeros_like(right_ref)
        right_ref[0:count] = high
        right_ref[count : 2 * count] = low
        right_ref[LANES : LANES + count] = high

    row = lax.broadcasted_iota(jnp.int32, (2 * LANES, 1), 0)
    mine = jnp.where(lax.rem(row, seqs) == sequence, 1.0, 0.0)
    right = (right_ref[...] * mine).astype(BF16)
    decay = decay_ref[pl.ds(sequence, 1), :]
    for group in range(heads // HPG):
        grown = dot(
            left_ref[group * group_width : (group + 1) * group_width],
            right[:, group * state_dim : (group + 1) * state_dim],
        )
        for head in range(HPG):
            index = group * HPG + head
            value = decay[:, index : index + 1] * state_ref[0, index] + grown[
                head * head_dim : (head + 1) * head_dim
            ]
            out_ref[0, index] = value
            half_ref[0, index] = value.astype(BF16)


def replay_state(accepted, path_dt, bias, a_log, conv_x, path_x, taps_x, conv_b, path_b, taps_b, state):
    seqs, heads, head_dim, state_dim = state.shape
    block = pl.BlockSpec((1, heads, head_dim, state_dim), lambda s: (s, 0, 0, 0))

    def full(array):
        return pl.BlockSpec(array.shape, lambda s: (0,) * array.ndim)

    small = [accepted, path_dt, bias, a_log, conv_x, path_x, taps_x, conv_b, path_b, taps_b]
    return pl.pallas_call(
        state_kernel,
        grid=(seqs,),
        out_shape=[
            jax.ShapeDtypeStruct(state.shape, F32),
            jax.ShapeDtypeStruct(state.shape, BF16),
        ],
        in_specs=[full(a) for a in small] + [block],
        out_specs=[block, block],
        scratch_shapes=[
            pltpu.VMEM((heads * head_dim, 2 * LANES), BF16),
            pltpu.VMEM((2 * LANES, path_b.shape[1]), F32),
            pltpu.VMEM((seqs, heads), F32),
        ],
        cost_estimate=cost(8),
        name="replay_state",
    )(*small, state)


def tree_kernel(parents_ref, accepted_ref, *refs):
    *inputs, links_ref, ancestry_ref, before_ref = refs
    seqs, props = parents_ref.shape
    nodes = seqs * props
    parents = parents_ref[...]
    parent = jnp.concatenate([parents[:, place : place + 1] for place in range(props)], axis=0)
    accepted = jnp.concatenate([accepted_ref[...]] * props, axis=0)
    row = lax.broadcasted_iota(jnp.int32, (nodes, nodes), 0)
    column = lax.broadcasted_iota(jnp.int32, (nodes, nodes), 1)
    own = lax.rem(lax.broadcasted_iota(jnp.int32, (nodes, 1), 0), seqs)
    target = jnp.where(parent >= 0, parent * seqs + own, -1)
    link = jnp.where(column == target, 1.0, 0.0)
    ancestry = link + jnp.where(row == column, 1.0, 0.0)
    link = link.astype(BF16)
    reach = link
    taps_count = inputs[2].shape[0]
    for distance in range(1, taps_count):
        links_ref[(distance - 1) * nodes : distance * nodes] = reach
        reach = dot(reach, link).astype(BF16)
    for _ in range(props.bit_length()):
        half = ancestry.astype(BF16)
        ancestry = jnp.minimum(dot(half, half), 1.0)
    ancestry_ref[...] = ancestry
    depth = jnp.sum(ancestry, axis=1, keepdims=True).astype(jnp.int32) - 1
    last = taps_count - 1

    def chosen(first, rows, distance):
        lane = lax.broadcasted_iota(jnp.int32, (nodes, rows), 1)
        wanted = accepted + last - distance + depth
        hit = (lane // seqs + first == wanted) & (lax.rem(lane, seqs) == own)
        return jnp.where(hit & (depth < distance), 1.0, 0.0).astype(BF16)

    conv_rows = inputs[0].shape[0]
    path_rows = inputs[1].shape[0]
    picks = [
        (chosen(0, conv_rows, d), chosen(conv_rows // seqs, path_rows, d))
        for d in range(1, taps_count)
    ]
    start = 0
    for which in range(0, len(inputs), 3):
        conv_ref, path_ref, taps_ref = inputs[which : which + 3]
        taps = taps_ref[...].astype(F32)
        total = 0.0
        for distance in range(1, taps_count):
            early, late = picks[distance - 1]
            found = dot(early, conv_ref[...]) + dot(late, path_ref[...])
            total = total + taps[last - distance : last - distance + 1] * found
        before_ref[:, start : start + conv_ref.shape[1]] = total
        start += conv_ref.shape[1]


def tree(parents, accepted, streams):
    nodes = parents.shape[0] * parents.shape[1]
    inputs = [array for stream in streams for array in stream]
    width = sum(stream[0].shape[1] for stream in streams)
    taps_count = streams[0][2].shape[0]
    return pl.pallas_call(
        tree_kernel,
        out_shape=[
            jax.ShapeDtypeStruct(((taps_count - 1) * nodes, nodes), BF16),
            jax.ShapeDtypeStruct((nodes, nodes), F32),
            jax.ShapeDtypeStruct((nodes, width), F32),
        ],
        in_specs=whole(len(inputs) + 2),
        out_specs=whole(3),
        cost_estimate=cost(4),
        name="tree",
    )(parents, accepted, *inputs)


def mix_kernel(
    seqs,
    width,
    local_heads,
    keep_bcr_ref,
    got_bcr_ref,
    keep_x_ref,
    got_x_ref,
    links_ref,
    ancestry_ref,
    before_ref,
    taps_x_ref,
    taps_b_ref,
    taps_c_ref,
    bias_ref,
    rate_ref,
    skip_ref,
    state_ref,
    out_ref,
    scale_ref,
    post_x_ref,
    post_b_ref,
    post_c_ref,
):
    nodes, inner = keep_x_ref.shape
    group_cols = taps_b_ref.shape[1]
    head_dim = inner // local_heads
    state_dim = state_ref.shape[3]
    groups = local_heads // HPG
    group_width = HPG * head_dim
    rate_start = 2 * group_cols
    extra = keep_bcr_ref[:, rate_start:].astype(F32) + got_bcr_ref[:, rate_start:].astype(F32)
    scale = lax.rsqrt(extra[:, local_heads : local_heads + 1] / width + EPS)
    scale_ref[...] = jnp.broadcast_to(scale, scale_ref.shape)

    ancestry = ancestry_ref[...]
    step = softplus((extra * scale).astype(BF16).astype(F32) + bias_ref[...])
    decayed = step * rate_ref[...]
    high, rest = split(decayed)
    middle, low = split(rest)
    parts = jnp.concatenate([high, middle, low], axis=1).astype(BF16)
    parts = dot(ancestry.astype(BF16), parts)
    decay = parts[:, :LANES] + parts[:, LANES : 2 * LANES] + parts[:, 2 * LANES :]
    grow = jnp.exp(decay)
    decay_t = decay.T
    step_t = step.T
    is_live = ancestry > 0.5

    def convolve(keep_ref, got_ref, taps_ref, source, start, target_ref):
        last = taps_ref.shape[0] - 1
        for lower in range(0, taps_ref.shape[1], CHUNK):
            span = slice(lower, lower + CHUNK)
            taken = slice(source + lower, source + lower + CHUNK)
            rows = keep_ref[:, taken].astype(F32) + got_ref[:, taken].astype(F32)
            rows = (rows * scale).astype(BF16)
            taps = taps_ref[:, span].astype(F32)
            found = dot(links_ref[...], rows)
            total = before_ref[:, start + lower : start + lower + CHUNK]
            total = total + taps[last : last + 1] * rows.astype(F32)
            for distance in range(1, last + 1):
                total = total + taps[last - distance : last - distance + 1] * found[
                    (distance - 1) * nodes : distance * nodes
                ]
            target_ref[:, span] = silu(total).astype(target_ref.dtype)

    convolve(keep_bcr_ref, got_bcr_ref, taps_b_ref, 0, inner, post_b_ref)
    convolve(keep_bcr_ref, got_bcr_ref, taps_c_ref, group_cols, inner + group_cols, post_c_ref)
    convolve(keep_x_ref, got_x_ref, taps_x_ref, 0, 0, post_x_ref)

    own = lax.rem(lax.broadcasted_iota(jnp.int32, (nodes, 1), 0), seqs)
    per_lanes = LANES // head_dim
    lane_head = lax.broadcasted_iota(jnp.int32, (nodes, LANES), 1) // head_dim
    for group in range(groups):
        rows_c = post_c_ref[:, group * state_dim : (group + 1) * state_dim]
        rows_b = post_b_ref[:, group * state_dim : (group + 1) * state_dim]
        scores = dot_nt(rows_c, rows_b)
        wide_c = rows_c.astype(F32)
        carried = 0.0
        for sequence in range(0, seqs, 2):
            left = jnp.concatenate(
                [
                    jnp.where(own == sequence + place, wide_c, 0.0).astype(BF16)
                    for place in range(2)
                ],
                axis=1,
            )
            right = jnp.concatenate(
                [
                    state_ref[sequence + place, group * HPG : (group + 1) * HPG].reshape(
                        group_width, state_dim
                    )
                    for place in range(2)
                ],
                axis=1,
            )
            carried = carried + dot_nt(left, right)
        for part in range(group_width // LANES):
            start = group * group_width + part * LANES
            rows_x = post_x_ref[:, start : start + LANES]
            half_x = rows_x.astype(BF16)
            within = 0.0
            growth = 0.0
            skip = 0.0
            for place in range(per_lanes):
                head = group * HPG + part * per_lanes + place
                gap = decay[:, head : head + 1] - decay_t[head : head + 1, :nodes]
                mixing = jnp.where(is_live, jnp.exp(jnp.where(is_live, gap, 0.0)), 0.0)
                mixing = (scores * mixing * step_t[head : head + 1, :nodes]).astype(BF16)
                within = jnp.where(lane_head == place, dot(mixing, half_x), within)
                growth = jnp.where(lane_head == place, grow[:, head : head + 1], growth)
                skip = jnp.where(lane_head == place, skip_ref[:, head : head + 1], skip)
            out_ref[:, start : start + LANES] = (
                carried[:, part * LANES : (part + 1) * LANES] * growth
                + within
                + skip * rows_x
            )


def mix(
    seqs,
    width,
    local_heads,
    keep_bcr,
    got_bcr,
    keep_x,
    got_x,
    links,
    ancestry,
    before,
    taps_x,
    taps_b,
    taps_c,
    bias,
    rate,
    skip,
    state,
):
    nodes, inner = keep_x.shape
    operands = [
        keep_bcr,
        got_bcr,
        keep_x,
        got_x,
        links,
        ancestry,
        before,
        taps_x,
        taps_b,
        taps_c,
        bias,
        rate,
        skip,
        state,
    ]
    return pl.pallas_call(
        functools.partial(mix_kernel, seqs, width, local_heads),
        out_shape=[
            jax.ShapeDtypeStruct((nodes, inner), F32),
            jax.ShapeDtypeStruct((nodes, LANES), F32),
        ],
        in_specs=whole(len(operands)),
        out_specs=whole(2),
        scratch_shapes=[
            pltpu.VMEM((nodes, inner), F32),
            pltpu.VMEM((nodes, taps_b.shape[1]), BF16),
            pltpu.VMEM((nodes, taps_c.shape[1]), BF16),
        ],
        cost_estimate=cost(8),
        name="mix",
    )(*operands)


def gate_kernel(group_width, keep_ref, got_ref, scale_ref, heads_ref, gain_ref, out_ref):
    scale = scale_ref[:, :1]
    for lower in range(0, out_ref.shape[1], group_width):
        span = slice(lower, lower + group_width)
        rows = keep_ref[:, span].astype(F32) + got_ref[:, span].astype(F32)
        rows = (rows * scale).astype(BF16).astype(F32)
        gated = heads_ref[:, span] * silu(rows)
        mean = jnp.sum(gated * gated, axis=1, keepdims=True) / group_width
        out_ref[:, span] = (gated * lax.rsqrt(mean + EPS) * gain_ref[:, span]).astype(BF16)


def gate(group_width, keep, got, scale, heads_out, gain):
    return pl.pallas_call(
        functools.partial(gate_kernel, group_width),
        out_shape=jax.ShapeDtypeStruct(heads_out.shape, BF16),
        in_specs=whole(5),
        out_specs=pl.BlockSpec(memory_space=VMEM),
        cost_estimate=cost(1),
        name="gate",
    )(keep, got, scale, heads_out, gain)


def swap_bit(array, bit, blocks):
    return lax.ppermute(array, "kv", [(i, i ^ (1 << bit)) for i in range(blocks)])


def after(value, *others):
    return lax.optimization_barrier((value, *others))[0]


def halving(keep, received, bit, blocks):
    half = keep.shape[0] // 2
    send = (keep[half:].astype(F32) + received[half:].astype(F32)).astype(BF16)

    def stay(*others):
        kept = after(keep, received, send, *others)
        got = after(received, keep, send, *others)
        return kept[:half].astype(F32) + got[:half].astype(F32)

    return send, swap_bit(send, bit, blocks), stay


def mixer(
    kv_count,
    tp_count,
    tokens,
    parents,
    accepted,
    state,
    conv_x,
    conv_b,
    conv_c,
    path_x,
    path_b,
    path_c,
    path_dt,
    gain_in,
    w_x,
    w_z,
    w_b,
    w_c,
    w_dt,
    dt_bias,
    a_log,
    d_skip,
    conv_wx,
    conv_wb,
    conv_wc,
    gain_out,
    w_out,
):
    seq_local = state.shape[0]
    proposals = parents.shape[1]
    heads_local = dt_bias.shape[0]
    head_dim = state.shape[2]
    width = gain_in.shape[0]
    tp_index = lax.axis_index("tp")
    kv_index = lax.axis_index("kv")
    slab_width = tokens.shape[2]
    rows_local = seq_local * proposals
    z_count = tp_count
    x_count = kv_count // z_count
    x_bits = list(range(log2(x_count)))
    z_bits = list(range(log2(x_count), log2(kv_count)))
    x_first = x_bits + z_bits
    z_first = z_bits + x_bits
    z_place = kv_index // x_count

    def by_position(array):
        return array.transpose(1, 0, 2).reshape(-1, array.shape[2])

    tokens_q = tokens.transpose(1, 0, 2).reshape(proposals, kv_count, seq_local, slab_width)
    gains = gain_in[None, :]
    half = kv_count // 2
    of_x = [flipped_bits(position, x_first) for position in range(kv_count)]
    of_z = [flipped_bits(position, z_first) for position in range(kv_count)]
    w_dt_t = w_dt.T
    bcr_args = (tp_count, gains, [w_b, w_c], w_dt_t)
    x_args = (tp_count, gains, [w_x])
    z_args = (tp_count, gains, [w_z])
    send_bcr = project(of_z[half:], tokens_q, *bcr_args)
    got_bcr = swap_bit(send_bcr, z_first[0], kv_count)
    send_x = project(of_x[half:], after(tokens_q, send_bcr), *x_args)
    got_x = swap_bit(send_x, x_first[0], kv_count)
    send_z = project(of_x[half:], after(tokens_q, send_x), *z_args)
    got_z = swap_bit(send_z, x_first[0], kv_count)
    keep_bcr = project(of_z[:half], after(tokens_q, send_z), *bcr_args)
    keep_x = project(of_x[:half], after(tokens_q, keep_bcr), *x_args)

    accepted = accepted[:, None]
    conv_x, conv_b, conv_c = by_position(conv_x), by_position(conv_b), by_position(conv_c)
    path_x, path_b, path_c = by_position(path_x), by_position(path_b), by_position(path_c)
    links, ancestry, before = tree(
        parents,
        after(accepted, keep_x),
        [(conv_x, path_x, conv_wx), (conv_b, path_b, conv_wb), (conv_c, path_c, conv_wc)],
    )
    sent_bcr, got_bcr, stay_bcr = halving(
        keep_bcr, after(got_bcr, links), z_first[1], kv_count
    )
    sent_x, got_x, stay_x = halving(keep_x, after(got_x, sent_bcr), x_first[1], kv_count)
    keep_z = project(of_x[:half], after(tokens_q, sent_x), *z_args)
    a_rate = -jnp.exp(a_log)
    new_state, half_state = replay_state(
        after(accepted, keep_z),
        by_position(path_dt),
        dt_bias[None, :],
        a_log[None, :],
        conv_x,
        path_x,
        conv_wx,
        conv_b,
        path_b,
        conv_wb,
        state,
    )
    keep_bcr = stay_bcr(keep_z)
    keep_x = stay_x(keep_z)
    sent_z, got_z, stay_z = halving(
        keep_z, after(got_z, half_state, keep_bcr, keep_x), x_first[1], kv_count
    )
    for place in range(2, len(x_first)):
        sent_x, got_x, stay_x = halving(
            keep_x, after(got_x, sent_z), x_first[place], kv_count
        )
        sent_bcr, got_bcr, stay_bcr = halving(
            keep_bcr, after(got_bcr, sent_x), z_first[place], kv_count
        )
        keep_x = stay_x(sent_bcr)
        keep_bcr = stay_bcr(sent_bcr)
        keep_z = stay_z(sent_bcr)
        sent_z, got_z, stay_z = halving(
            keep_z, after(got_z, keep_x, keep_bcr), x_first[place], kv_count
        )
    got_x = after(got_x, sent_z)
    got_bcr = after(got_bcr, sent_z)
    keep_z = stay_z(sent_z)

    def padded(values):
        return jnp.pad(values, (0, LANES - heads_local))[None, :]

    heads_out, row_scale = mix(
        seq_local,
        width,
        heads_local,
        keep_bcr,
        got_bcr,
        keep_x,
        got_x,
        links,
        ancestry,
        before,
        conv_wx,
        conv_wb,
        conv_wc,
        padded(dt_bias),
        padded(a_rate),
        d_skip[None, :],
        half_state,
    )
    gated = gate(HPG * head_dim, keep_z, got_z, row_scale, heads_out, gain_out[None, :])

    w_out = after(w_out, sent_bcr, sent_x)
    w_pieces = [w_out]
    for bit in x_bits:
        w_pieces = w_pieces + [swap_bit(piece, bit, kv_count) for piece in w_pieces]
    w_pieces = [after(piece, gated) for piece in w_pieces]
    for bit in x_bits:
        flip = ((kv_index >> bit) & 1) == 1
        w_pieces = [
            jnp.where(flip, w_pieces[place ^ (1 << bit)], w_pieces[place])
            for place in range(x_count)
        ]
    w_block = jnp.concatenate(w_pieces, axis=1)

    pieces = {0: gated}
    for bit in z_bits[::-1]:
        for place in list(pieces):
            pieces[place | (1 << (bit - len(x_bits)))] = swap_bit(pieces[place], bit, kv_count)
    terms = [dot(pieces[place], w_block).astype(BF16) for place in range(z_count)]
    core_flip = ((tp_index ^ z_place) & 1) == 1
    sent = []
    kept = []
    for place in range(0, z_count, 2):
        sent.append(jnp.where(core_flip, terms[place], terms[place + 1]))
        kept.append(jnp.where(core_flip, terms[place + 1], terms[place]))
    swapped = lax.ppermute(
        jnp.concatenate(sent, axis=0), "tp", [(i, i ^ 1) for i in range(tp_count)]
    )
    half = z_count // 2
    paired = (jnp.concatenate(kept, axis=0).astype(F32) + swapped.astype(F32)).astype(
        BF16
    ).reshape(half, rows_local, -1)
    total = 0.0
    for shift in range(half):
        block = (tp_index >> 1) ^ (z_place >> 1) ^ shift
        route = []
        for z in range(z_count):
            for x in range(x_count):
                for t in range(tp_count):
                    z_to = (((t >> 1) ^ shift) << 1) | (t & 1)
                    route.append(
                        ((z * x_count + x) * tp_count + t, (z_to * x_count + x) * tp_count + z)
                    )
        piece = lax.dynamic_index_in_dim(paired, block, 0, keepdims=False)
        total = total + lax.ppermute(piece, ("kv", "tp"), route).astype(F32)
    mixed = total.astype(BF16).reshape(proposals, seq_local, -1).transpose(1, 0, 2)
    return (mixed, new_state)


def solution(mesh):
    return jax.shard_map(
        functools.partial(mixer, mesh.shape["kv"], mesh.shape["tp"]),
        mesh=mesh,
        in_specs=(
            P(None, None, "kv"),
            P("kv", None),
            P("kv"),
            P("kv", "tp", None, None),
            P("kv", None, "tp"),
            P("kv", None, "tp"),
            P("kv", None, "tp"),
            P("kv", None, "tp"),
            P("kv", None, "tp"),
            P("kv", None, "tp"),
            P("kv", None, "tp"),
            P(),
            P("kv", "tp"),
            P("kv", "tp"),
            P("kv", "tp"),
            P("kv", "tp"),
            P(),
            P("tp"),
            P("tp"),
            P("tp"),
            P(None, "tp"),
            P(None, "tp"),
            P(None, "tp"),
            P("tp"),
            P("tp", "kv"),
        ),
        out_specs=(P("kv", None, "tp"), P("kv", "tp", None, None)),
        check_vma=False,
    )
```

profile of v0, /device:TPU:4, one launch (start us, length us, event | category | flops | bytes accessed | tf_op | source)
XLA Modules:
  0.0 113.6 jit_solution(18167536262701792637)
XLA Ops:
  0.6 3.5 %project.6 = bf16[384,1152]{1,0:T(8,128)(2,1)} custom-call(bf16[12,8,8,512]{3,2,1,0:T(8,128)(2,1)} %bitcast.48, f32[1,4096]{1,0:T(1,128)} %bitcast.57, bf16[64,4096]{1,0:T(8,128)(2,1)} %bitcast.54, bf16[512,512]{1,0:T(8,128)(2,1)} %refs_1_.3, bf16[512,512]{1,0:T(8,128)(2,1)} %refs_2_.4), custom_call_target="tpu_custom_call" | custom-call | flops 8000000 | bytes 1024 | tf_op jit(solution)/shard_map/project/pallas_call | solution.py:109
  4.1 1.6 %collective-permute-start.1 = (bf16[384,1152]{1,0:T(8,128)(2,1)}, bf16[384,1152]{1,0:T(8,128)(2,1)S(1)}, u32[]{:S(2)}, u32[]{:S(2)}) collective-permute-start(bf16[384,1152]{1,0:T(8,128)(2,1)} %project.6), channel_id=1, source_target_pairs={{0,8},{4,12},{8,0},{12,4},{16,24},{20,28},{24,16},{28,20},{1,9},{5... | collective-permute-start | bytes 2654216 | tf_op jit(solution)/shard_map/ppermute | solution.py:502
  5.7 3.0 %project.7 = bf16[384,1024]{1,0:T(8,128)(2,1)} custom-call(bf16[12,8,8,512]{3,2,1,0:T(8,128)(2,1)} %bitcast.49, f32[1,4096]{1,0:T(1,128)} %bitcast.58, bf16[512,1024]{1,0:T(8,128)(2,1)} %refs_0_.6), custom_call_target="tpu_custom_call" | custom-call | flops 8000000 | bytes 1024 | tf_op jit(solution)/shard_map/project/pallas_call | solution.py:109
  8.7 1.5 %collective-permute-start = (bf16[384,1024]{1,0:T(8,128)(2,1)}, bf16[384,1024]{1,0:T(8,128)(2,1)S(1)}, u32[]{:S(2)}, u32[]{:S(2)}) collective-permute-start(bf16[384,1024]{1,0:T(8,128)(2,1)} %project.7), channel_id=1, source_target_pairs={{0,4},{4,0},{8,12},{12,8},{16,20},{20,16},{24,28},{28,24},{1,5},{5... | collective-permute-start | bytes 2359304 | tf_op jit(solution)/shard_map/ppermute | solution.py:502
  10.1 3.0 %project.8 = bf16[384,1024]{1,0:T(8,128)(2,1)} custom-call(bf16[12,8,8,512]{3,2,1,0:T(8,128)(2,1)} %bitcast.50, f32[1,4096]{1,0:T(1,128)} %bitcast.59, bf16[512,1024]{1,0:T(8,128)(2,1)} %refs_0_.7), custom_call_target="tpu_custom_call" | custom-call | flops 8000000 | bytes 1024 | tf_op jit(solution)/shard_map/project/pallas_call | solution.py:109
  13.6 3.5 %project.9 = bf16[384,1152]{1,0:T(8,128)(2,1)} custom-call(bf16[12,8,8,512]{3,2,1,0:T(8,128)(2,1)} %bitcast.51, f32[1,4096]{1,0:T(1,128)} %bitcast.60, bf16[64,4096]{1,0:T(8,128)(2,1)} %bitcast.55, bf16[512,512]{1,0:T(8,128)(2,1)} %refs_1_.3, bf16[512,512]{1,0:T(8,128)(2,1)} %refs_2_.4), custom_call_target="tpu_custom_call" | custom-call | flops 8000000 | bytes 1024 | tf_op jit(solution)/shard_map/project/pallas_call | solution.py:109
  17.2 3.0 %project.10 = bf16[384,1024]{1,0:T(8,128)(2,1)} custom-call(bf16[12,8,8,512]{3,2,1,0:T(8,128)(2,1)} %bitcast.52, f32[1,4096]{1,0:T(1,128)} %bitcast.61, bf16[512,1024]{1,0:T(8,128)(2,1)} %refs_0_.6), custom_call_target="tpu_custom_call" | custom-call | flops 8000000 | bytes 1024 | tf_op jit(solution)/shard_map/project/pallas_call | solution.py:109
  20.8 3.4 %tree.1 = (bf16[288,96]{1,0:T(8,128)(2,1)}, f32[96,96]{1,0:T(8,128)}, f32[96,2048]{1,0:T(8,128)}) custom-call(s32[8,12]{1,0:T(8,128)} %parents_ref.1, s32[8,1]{1,0:T(8,128)} %copy.27.accepted_ref, bf16[24,1024]{1,0:T(8,128)(2,1)} %bitcast.65, bf16[48,1024]{1,0:T(8,128)(2,1)} %bitcast.63, bf16[4,1024]{1,0:T(4,128)(2,1)} %taps_x_ref.3, ...), custom_call_target="tpu_custom_call" | custom-call | flops 16000000 | bytes 1024 | tf_op jit(solution)/shard_map/tree/pallas_call | solution.py:293
  24.8 0.9 collective-permute-done.1
  26.6 2.7 %collective-permute-done = bf16[384,1024]{1,0:T(8,128)(2,1)S(1)} collective-permute-done((bf16[384,1024]{1,0:T(8,128)(2,1)}, bf16[384,1024]{1,0:T(8,128)(2,1)S(1)}, u32[]{:S(2)}, u32[]{:S(2)}) %collective-permute-start) | collective-permute-done | bytes 786464 | tf_op jit(solution)/shard_map/ppermute | solution.py:502
  29.3 2.1 %add_convert_fusion.3 = bf16[192,1024]{1,0:T(8,128)(2,1)} fusion(bf16[384,1024]{1,0:T(8,128)(2,1)} %project.10, bf16[384,1024]{1,0:T(8,128)(2,1)S(1)} %collective-permute-done), kind=kLoop, calls=%fused_computation.13 | loop fusion | flops 786432 | bytes 1179648 | tf_op jit(solution)/shard_map/convert_element_type | solution.py:511
  31.4 3.0 %project.11 = bf16[384,1024]{1,0:T(8,128)(2,1)} custom-call(bf16[12,8,8,512]{3,2,1,0:T(8,128)(2,1)} %bitcast.53, f32[1,4096]{1,0:T(1,128)} %bitcast.62, bf16[512,1024]{1,0:T(8,128)(2,1)} %refs_0_.7), custom_call_target="tpu_custom_call" | custom-call | flops 8000000 | bytes 1024 | tf_op jit(solution)/shard_map/project/pallas_call | solution.py:109
  34.8 2.6 %collective-permute-start.3 = (bf16[192,1152]{1,0:T(8,128)(2,1)}, bf16[192,1152]{1,0:T(8,128)(2,1)}, u32[]{:S(2)}, u32[]{:S(2)}) collective-permute-start(bf16[192,1152]{1,0:T(8,128)(2,1)} %add_convert_fusion), channel_id=1, source_target_pairs={{0,16},{4,20},{8,24},{12,28},{16,0},{20,4},{24,8},{28,12},{1,17},{... | collective-permute-start | bytes 1327112 | tf_op jit(solution)/shard_map/ppermute | solution.py:502
  38.1 8.6 %replay_state.1 = (f32[8,16,64,128]{3,2,1,0:T(8,128)}, bf16[8,16,64,128]{3,2,1,0:T(8,128)(2,1)}) custom-call(s32[8,1]{1,0:T(8,128)} %copy.28.accepted_ref, bf16[48,16]{1,0:T(8,128)(2,1)} %bitcast.73, f32[1,16]{1,0:T(1,128)} %bitcast.75, f32[1,16]{1,0:T(1,128)} %bitcast.78, bf16[24,1024]{1,0:T(8,128)(2,1)} %bitcast.66, bf16[48,1024]{1,0:T(8,128)(2,1)} %bitcast.64, ...), custom_call_target="tpu_custom_call" | custom-call | flops 32000000 | bytes 1024 | tf_op jit(solution)/shard_map/replay_state/pallas_call | solution.py:218
  46.8 1.2 %convert_add_fusion.2 = f32[192,1024]{1,0:T(8,128)S(1)} fusion(bf16[384,1024]{1,0:T(8,128)(2,1)} %copy-done.4, bf16[384,1024]{1,0:T(8,128)(2,1)S(1)} %copy-done.2), kind=kLoop, calls=%fused_computation.12 | loop fusion | flops 589824 | bytes 1572864 | tf_op jit(solution)/shard_map/add | solution.py:516
  48.2 1.7 %collective-permute-start.5 = (bf16[192,1024]{1,0:T(8,128)(2,1)S(1)}, bf16[192,1024]{1,0:T(8,128)(2,1)S(1)}, u32[]{:S(2)}, u32[]{:S(2)}) collective-permute-start(bf16[192,1024]{1,0:T(8,128)(2,1)S(1)} %add_convert_fusion.2), channel_id=1, source_target_pairs={{0,8},{4,12},{8,0},{12,4},{16,24},{20,28},{24,16},{28,20},{1,9},{5... | collective-permute-start | bytes 1179656 | tf_op jit(solution)/shard_map/ppermute | solution.py:502
  49.9 3.9 %collective-permute-done.4 = bf16[192,1024]{1,0:T(8,128)(2,1)} collective-permute-done((bf16[192,1024]{1,0:T(8,128)(2,1)}, bf16[192,1024]{1,0:T(8,128)(2,1)}, u32[]{:S(2)}, u32[]{:S(2)}) %collective-permute-start.4) | collective-permute-done | bytes 393248 | tf_op jit(solution)/shard_map/ppermute | solution.py:502
  53.8 1.0 fusion.2
  55.1 1.0 fusion
  56.1 1.6 %collective-permute-start.7 = (bf16[96,1152]{1,0:T(8,128)(2,1)S(1)}, bf16[96,1152]{1,0:T(8,128)(2,1)S(1)}, u32[]{:S(2)}, u32[]{:S(2)}) collective-permute-start(bf16[96,1152]{1,0:T(8,128)(2,1)S(1)} %fusion), channel_id=1, source_target_pairs={{0,4},{4,0},{8,12},{12,8},{16,20},{20,16},{24,28},{28,24},{1,5},{5... | collective-permute-start | bytes 663560 | tf_op jit(solution)/shard_map/ppermute | solution.py:502
  58.2 1.7 %convert_add_fusion.3.keep_bcr_ref = f32[96,1152]{1,0:T(8,128)} fusion(f32[192,1152]{1,0:T(8,128)S(1)} %convert_add_fusion, bf16[192,1152]{1,0:T(8,128)(2,1)} %collective-permute-done.3), kind=kLoop, calls=%fused_computation.16 | loop fusion | flops 221184 | bytes 1105920 | tf_op jit(solution)/shard_map/add | solution.py:516
  59.9 1.7 %convert_add_fusion.5.keep_x_ref = f32[96,1024]{1,0:T(8,128)} fusion(f32[192,1024]{1,0:T(8,128)S(1)} %convert_add_fusion.2, bf16[192,1024]{1,0:T(8,128)(2,1)} %collective-permute-done.4), kind=kLoop, calls=%fused_computation.24 | loop fusion | flops 196608 | bytes 983040 | tf_op jit(solution)/shard_map/add | solution.py:516
  61.6 3.4 %collective-permute-done.5 = bf16[192,1024]{1,0:T(8,128)(2,1)S(1)} collective-permute-done((bf16[192,1024]{1,0:T(8,128)(2,1)S(1)}, bf16[192,1024]{1,0:T(8,128)(2,1)S(1)}, u32[]{:S(2)}, u32[]{:S(2)}) %collective-permute-start.5) | collective-permute-done | bytes 393248 | tf_op jit(solution)/shard_map/ppermute | solution.py:502
  67.5 4.9 %mix.1 = (f32[96,1024]{1,0:T(8,128)}, f32[96,128]{1,0:T(8,128)}) custom-call(f32[96,1152]{1,0:T(8,128)} %convert_add_fusion.3.keep_bcr_ref, bf16[96,1152]{1,0:T(8,128)(2,1)} %copy-done.5, f32[96,1024]{1,0:T(8,128)} %convert_add_fusion.5.keep_x_ref, bf16[96,1024]{1,0:T(8,128)(2,1)} %copy-done.6, bf16[288,96]{1,0:T(8,128)(2,1)} %get-tuple-element.44.links_ref, ...), custom_call_target="tpu_custom_call" | custom-call | flops 32000000 | bytes 1024 | tf_op jit(solution)/shard_map/mix/pallas_call | solution.py:461
  72.4 3.1 %collective-permute-done.6.got_ref = bf16[96,1024]{1,0:T(8,128)(2,1)S(1)} collective-permute-done((bf16[96,1024]{1,0:T(8,128)(2,1)S(1)}, bf16[96,1024]{1,0:T(8,128)(2,1)S(1)}, u32[]{:S(2)}, u32[]{:S(2)}) %collective-permute-start.6) | collective-permute-done | bytes 196640 | tf_op jit(solution)/shard_map/ppermute | solution.py:502
  76.2 2.2 %gate.1 = bf16[96,1024]{1,0:T(8,128)(2,1)} custom-call(f32[96,1024]{1,0:T(8,128)} %convert_add_fusion.4.keep_ref, bf16[96,1024]{1,0:T(8,128)(2,1)} %copy-done.8, f32[96,128]{1,0:T(8,128)} %get-tuple-element.70.scale_ref, f32[96,1024]{1,0:T(8,128)} %get-tuple-element.71.heads_ref, f32[1,1024]{1,0:T(1,128)} %bitcast.74), custom_call_target="tpu_custom_call" | custom-call | flops 4000000 | bytes 1024 | tf_op jit(solution)/shard_map/gate/pallas_call | solution.py:491
  78.4 2.2 %collective-permute-start.9 = (bf16[96,1024]{1,0:T(8,128)(2,1)}, bf16[96,1024]{1,0:T(8,128)(2,1)S(1)}, u32[]{:S(2)}, u32[]{:S(2)}) collective-permute-start(bf16[96,1024]{1,0:T(8,128)(2,1)} %gate.1), channel_id=1, source_target_pairs={{0,8},{4,12},{8,0},{12,4},{16,24},{20,28},{24,16},{28,20},{1,9},{5... | collective-permute-start | bytes 589832 | tf_op jit(solution)/shard_map/ppermute | solution.py:502
  80.6 8.6 %collective-permute-done.11 = bf16[96,1024]{1,0:T(8,128)(2,1)S(1)} collective-permute-done((bf16[96,1024]{1,0:T(8,128)(2,1)}, bf16[96,1024]{1,0:T(8,128)(2,1)S(1)}, u32[]{:S(2)}, u32[]{:S(2)}) %collective-permute-start.11) | collective-permute-done | bytes 196640 | tf_op jit(solution)/shard_map/ppermute | solution.py:502
  90.9 5.2 %collective-permute-done.12 = bf16[96,1024]{1,0:T(8,128)(2,1)S(1)} collective-permute-done((bf16[96,1024]{1,0:T(8,128)(2,1)S(1)}, bf16[96,1024]{1,0:T(8,128)(2,1)S(1)}, u32[]{:S(2)}, u32[]{:S(2)}) %collective-permute-start.12) | collective-permute-done | bytes 196640 | tf_op jit(solution)/shard_map/ppermute | solution.py:502
  96.6 1.7 %collective-permute-done.13 = bf16[192,1024]{1,0:T(8,128)(2,1)S(1)} collective-permute-done((bf16[192,1024]{1,0:T(8,128)(2,1)S(1)}, bf16[192,1024]{1,0:T(8,128)(2,1)S(1)}, u32[]{:S(2)}, u32[]{:S(2)}) %collective-permute-start.13) | collective-permute-done | bytes 393248 | tf_op jit(solution)/shard_map/ppermute | solution.py:685
  98.5 3.1 %collective-permute-start.14 = (bf16[96,1024]{1,0:T(8,128)(2,1)S(1)}, bf16[96,1024]{1,0:T(8,128)(2,1)S(1)}, u32[]{:S(2)}, u32[]{:S(2)}) collective-permute-start(bf16[96,1024]{1,0:T(8,128)(2,1)S(1)} %get-tuple-element.78), channel_id=1, source_target_pairs={{0,0},{1,8},{2,16},{3,24},{4,4},{5,12},{6,20},{7,28},{8,1},{9,9},{... | collective-permute-start | bytes 589832 | tf_op jit(solution)/shard_map/ppermute | solution.py:704
  101.7 10.8 %collective-permute-done.14 = bf16[96,1024]{1,0:T(8,128)(2,1)S(1)} collective-permute-done((bf16[96,1024]{1,0:T(8,128)(2,1)S(1)}, bf16[96,1024]{1,0:T(8,128)(2,1)S(1)}, u32[]{:S(2)}, u32[]{:S(2)}) %collective-permute-start.14) | collective-permute-done | bytes 196640 | tf_op jit(solution)/shard_map/ppermute | solution.py:704
  (59 shorter events, 11.5 us)
Async XLA Ops:
  4.1 21.6 %collective-permute-start.1 = (bf16[384,1152]{1,0:T(8,128)(2,1)}, bf16[384,1152]{1,0:T(8,128)(2,1)S(1)}, u32[]{:S(2)}, u32[]{:S(2)}) collective-permute-start(bf16[384,1152]{1,0:T(8,128)(2,1)} %project.6), channel_id=1, source_target_pairs={{0,8},{4,12},{8,0},{12,4},{16,24},{20,28},{24,16},{28,20},{1,9},{5... | collective-permute-start | bytes 2654216 | tf_op jit(solution)/shard_map/ppermute | solution.py:502
  8.7 20.6 %collective-permute-start = (bf16[384,1024]{1,0:T(8,128)(2,1)}, bf16[384,1024]{1,0:T(8,128)(2,1)S(1)}, u32[]{:S(2)}, u32[]{:S(2)}) collective-permute-start(bf16[384,1024]{1,0:T(8,128)(2,1)} %project.7), channel_id=1, source_target_pairs={{0,4},{4,0},{8,12},{12,8},{16,20},{20,16},{24,28},{28,24},{1,5},{5... | collective-permute-start | bytes 2359304 | tf_op jit(solution)/shard_map/ppermute | solution.py:502
  13.1 35.0 %collective-permute-start.2 = (bf16[384,1024]{1,0:T(8,128)(2,1)}, bf16[384,1024]{1,0:T(8,128)(2,1)S(1)}, u32[]{:S(2)}, u32[]{:S(2)}) collective-permute-start(bf16[384,1024]{1,0:T(8,128)(2,1)} %project.8), channel_id=1, source_target_pairs={{0,4},{4,0},{8,12},{12,8},{16,20},{20,16},{24,28},{28,24},{1,5},{5... | collective-permute-start | bytes 2359304 | tf_op jit(solution)/shard_map/ppermute | solution.py:502
  17.1 3.0 %copy-start.10 = (s32[8]{0:T(128)S(1)}, s32[8]{0:T(128)}, u32[]{:S(2)}) copy-start(s32[8]{0:T(128)} %param.27) | copy-start | bytes 100
  17.1 7.1 %copy-start.11 = (f32[16]{0:T(128)S(1)}, f32[16]{0:T(128)}, u32[]{:S(2)}) copy-start(f32[16]{0:T(128)} %param.43) | copy-start | bytes 196
  17.1 7.1 %copy-start.9 = (f32[16]{0:T(128)S(1)}, f32[16]{0:T(128)}, u32[]{:S(2)}) copy-start(f32[16]{0:T(128)} %param.42) | copy-start | bytes 196
  17.2 8.6 %copy-start = (bf16[384,1152]{1,0:T(8,128)(2,1)S(1)}, bf16[384,1152]{1,0:T(8,128)(2,1)}, u32[]{:S(2)}) copy-start(bf16[384,1152]{1,0:T(8,128)(2,1)} %project.9) | copy-start | bytes 2654212
  29.3 8.8 %copy-start.4 = (bf16[384,1024]{1,0:T(8,128)(2,1)}, bf16[384,1024]{1,0:T(8,128)(2,1)S(1)}, u32[]{:S(2)}) copy-start(bf16[384,1024]{1,0:T(8,128)(2,1)S(1)} %collective-permute-done) | copy-start | bytes 2359300
  34.4 19.4 %collective-permute-start.4 = (bf16[192,1024]{1,0:T(8,128)(2,1)}, bf16[192,1024]{1,0:T(8,128)(2,1)}, u32[]{:S(2)}, u32[]{:S(2)}) collective-permute-start(bf16[192,1024]{1,0:T(8,128)(2,1)} %add_convert_fusion.3), channel_id=1, source_target_pairs={{0,8},{4,12},{8,0},{12,4},{16,24},{20,28},{24,16},{28,20},{1,9},{5... | collective-permute-start | bytes 1179656 | tf_op jit(solution)/shard_map/ppermute | solution.py:502
  34.8 20.3 %collective-permute-start.3 = (bf16[192,1152]{1,0:T(8,128)(2,1)}, bf16[192,1152]{1,0:T(8,128)(2,1)}, u32[]{:S(2)}, u32[]{:S(2)}) collective-permute-start(bf16[192,1152]{1,0:T(8,128)(2,1)} %add_convert_fusion), channel_id=1, source_target_pairs={{0,16},{4,20},{8,24},{12,28},{16,0},{20,4},{24,8},{28,12},{1,17},{... | collective-permute-start | bytes 1327112 | tf_op jit(solution)/shard_map/ppermute | solution.py:502
  38.1 8.7 %copy-start.2 = (bf16[384,1024]{1,0:T(8,128)(2,1)S(1)}, bf16[384,1024]{1,0:T(8,128)(2,1)}, u32[]{:S(2)}) copy-start(bf16[384,1024]{1,0:T(8,128)(2,1)} %project.10) | copy-start | bytes 2359300
  46.7 1.3 %copy-start.1 = (bf16[384,1024]{1,0:T(8,128)(2,1)S(1)}, bf16[384,1024]{1,0:T(8,128)(2,1)}, u32[]{:S(2)}) copy-start(bf16[384,1024]{1,0:T(8,128)(2,1)} %project.11) | copy-start | bytes 2359300
  46.8 10.8 %copy-start.3 = (bf16[1024,512]{1,0:T(8,128)(2,1)S(1)}, bf16[1024,512]{1,0:T(8,128)(2,1)}, u32[]{:S(2)}) copy-start(bf16[1024,512]{1,0:T(8,128)(2,1)} %param.49) | copy-start | bytes 3145732
  48.2 16.8 %collective-permute-start.5 = (bf16[192,1024]{1,0:T(8,128)(2,1)S(1)}, bf16[192,1024]{1,0:T(8,128)(2,1)S(1)}, u32[]{:S(2)}, u32[]{:S(2)}) collective-permute-start(bf16[192,1024]{1,0:T(8,128)(2,1)S(1)} %add_convert_fusion.2), channel_id=1, source_target_pairs={{0,8},{4,12},{8,0},{12,4},{16,24},{20,28},{24,16},{28,20},{1,9},{5... | collective-permute-start | bytes 1179656 | tf_op jit(solution)/shard_map/ppermute | solution.py:502
  54.8 12.0 %collective-permute-start.8 = (bf16[96,1024]{1,0:T(8,128)(2,1)S(1)}, bf16[96,1024]{1,0:T(8,128)(2,1)S(1)}, u32[]{:S(2)}, u32[]{:S(2)}) collective-permute-start(bf16[96,1024]{1,0:T(8,128)(2,1)S(1)} %fusion.2), channel_id=1, source_target_pairs={{0,16},{4,20},{8,24},{12,28},{16,0},{20,4},{24,8},{28,12},{1,17},{... | collective-permute-start | bytes 589832 | tf_op jit(solution)/shard_map/ppermute | solution.py:502
  56.1 10.7 %collective-permute-start.7 = (bf16[96,1152]{1,0:T(8,128)(2,1)S(1)}, bf16[96,1152]{1,0:T(8,128)(2,1)S(1)}, u32[]{:S(2)}, u32[]{:S(2)}) collective-permute-start(bf16[96,1152]{1,0:T(8,128)(2,1)S(1)} %fusion), channel_id=1, source_target_pairs={{0,4},{4,0},{8,12},{12,8},{16,20},{20,16},{24,28},{28,24},{1,5},{5... | collective-permute-start | bytes 663560 | tf_op jit(solution)/shard_map/ppermute | solution.py:502
  57.6 31.6 %collective-permute-start.10 = (bf16[1024,512]{1,0:T(8,128)(2,1)S(1)}, bf16[1024,512]{1,0:T(8,128)(2,1)S(1)}, u32[]{:S(2)}, u32[]{:S(2)}) collective-permute-start(bf16[1024,512]{1,0:T(8,128)(2,1)S(1)} %copy-done.3), channel_id=1, source_target_pairs={{0,4},{4,0},{8,12},{12,8},{16,20},{20,16},{24,28},{28,24},{1,5},{5... | collective-permute-start | bytes 3145736 | tf_op jit(solution)/shard_map/ppermute | solution.py:502
  65.2 10.3 %collective-permute-start.6 = (bf16[96,1024]{1,0:T(8,128)(2,1)S(1)}, bf16[96,1024]{1,0:T(8,128)(2,1)S(1)}, u32[]{:S(2)}, u32[]{:S(2)}) collective-permute-start(bf16[96,1024]{1,0:T(8,128)(2,1)S(1)} %fusion.1), channel_id=1, source_target_pairs={{0,16},{4,20},{8,24},{12,28},{16,0},{20,4},{24,8},{28,12},{1,17},{... | collective-permute-start | bytes 589832 | tf_op jit(solution)/shard_map/ppermute | solution.py:502
  66.7 0.8 copy-start.6
  66.8 0.8 copy-start.5
  75.5 0.7 copy-start.8
  78.4 10.8 %collective-permute-start.11 = (bf16[96,1024]{1,0:T(8,128)(2,1)}, bf16[96,1024]{1,0:T(8,128)(2,1)S(1)}, u32[]{:S(2)}, u32[]{:S(2)}) collective-permute-start(bf16[96,1024]{1,0:T(8,128)(2,1)} %gate.1), channel_id=1, source_target_pairs={{0,16},{4,20},{8,24},{12,28},{16,0},{20,4},{24,8},{28,12},{1,17},{... | collective-permute-start | bytes 589832 | tf_op jit(solution)/shard_map/ppermute | solution.py:502
  78.4 11.0 %copy-start.7 = (bf16[96,1024]{1,0:T(8,128)(2,1)S(1)}, bf16[96,1024]{1,0:T(8,128)(2,1)}, u32[]{:S(2)}) copy-start(bf16[96,1024]{1,0:T(8,128)(2,1)} %gate.1) | copy-start | bytes 589828
  78.4 11.5 %collective-permute-start.9 = (bf16[96,1024]{1,0:T(8,128)(2,1)}, bf16[96,1024]{1,0:T(8,128)(2,1)S(1)}, u32[]{:S(2)}, u32[]{:S(2)}) collective-permute-start(bf16[96,1024]{1,0:T(8,128)(2,1)} %gate.1), channel_id=1, source_target_pairs={{0,8},{4,12},{8,0},{12,4},{16,24},{20,28},{24,16},{28,20},{1,9},{5... | collective-permute-start | bytes 589832 | tf_op jit(solution)/shard_map/ppermute | solution.py:502
  89.3 6.8 %collective-permute-start.12 = (bf16[96,1024]{1,0:T(8,128)(2,1)S(1)}, bf16[96,1024]{1,0:T(8,128)(2,1)S(1)}, u32[]{:S(2)}, u32[]{:S(2)}) collective-permute-start(bf16[96,1024]{1,0:T(8,128)(2,1)S(1)} %collective-permute-done.11), channel_id=1, source_target_pairs={{0,8},{4,12},{8,0},{12,4},{16,24},{20,28},{24,16},{28,20},{1,9},{5... | collective-permute-start | bytes 589832 | tf_op jit(solution)/shard_map/ppermute | solution.py:502
  96.5 1.8 %collective-permute-start.13 = (bf16[192,1024]{1,0:T(8,128)(2,1)S(1)}, bf16[192,1024]{1,0:T(8,128)(2,1)S(1)}, u32[]{:S(2)}, u32[]{:S(2)}) collective-permute-start(bf16[192,1024]{1,0:T(8,128)(2,1)S(1)} %pad_maximum_fusion.1), channel_id=1, source_target_pairs={{0,1},{1,0},{2,3},{3,2},{4,5},{5,4},{6,7},{7,6},{8,9},{9,8},{10,11... | collective-permute-start | bytes 1179656 | tf_op jit(solution)/shard_map/ppermute | solution.py:685
  98.5 13.9 %collective-permute-start.14 = (bf16[96,1024]{1,0:T(8,128)(2,1)S(1)}, bf16[96,1024]{1,0:T(8,128)(2,1)S(1)}, u32[]{:S(2)}, u32[]{:S(2)}) collective-permute-start(bf16[96,1024]{1,0:T(8,128)(2,1)S(1)} %get-tuple-element.78), channel_id=1, source_target_pairs={{0,0},{1,8},{2,16},{3,24},{4,4},{5,12},{6,20},{7,28},{8,1},{9,9},{... | collective-permute-start | bytes 589832 | tf_op jit(solution)/shard_map/ppermute | solution.py:704
  101.6 11.3 %collective-permute-start.15 = (bf16[96,1024]{1,0:T(8,128)(2,1)S(1)}, bf16[96,1024]{1,0:T(8,128)(2,1)S(1)}, u32[]{:S(2)}, u32[]{:S(2)}) collective-permute-start(bf16[96,1024]{1,0:T(8,128)(2,1)S(1)} %get-tuple-element.79), channel_id=1, source_target_pairs={{0,16},{1,24},{2,0},{3,8},{4,20},{5,28},{6,4},{7,12},{8,17},{9,25}... | collective-permute-start | bytes 589832 | tf_op jit(solution)/shard_map/ppermute | solution.py:704
where the time goes:
time: 114 us
  waiting for transfers between devices  40.7 us (36%)
  Pallas kernels  38.1 us (33%)
  starting transfers between devices  16.9 us (15%)
  other arithmetic  11.8 us (10%)
  local copies, waits for them, and re-layouts  3.37 us (3%)
  matrix products  1.89 us (2%)
    ppermute x13, waiting for transfers between devices, swap_bit(): return lax.ppermute(array, 'kv', [(i, i ^ 1 << bit) for i in range(blocks)])  27.8 us
    pallas_call x6, Pallas kernels, project(): pl.pallas_call(functools.partial(project_kernel, tuple(differences), w_dt...  18.9 us
    ppermute x13, starting transfers between devices, swap_bit(): return lax.ppermute(array, 'kv', [(i, i ^ 1 << bit) for i in range(blocks)])  13.7 us
    ppermute x2, waiting for transfers between devices, mixer(): total = total + lax.ppermute(piece, ('kv', 'tp'), route).astype(F32)  11.2 us
    pallas_call x1, Pallas kernels, replay_state(): pl.pallas_call(state_kernel, grid=(seqs,), out_shape=[jax.ShapeDtypeStruc...  8.63 us
    add x6, other arithmetic, stay(): return kept[:half].astype(F32) + got[:half].astype(F32)  5.67 us
    convert_element_type x6, other arithmetic, halving(): send = (keep[half:].astype(F32) + received[half:].astype(F32)).astype(BF16)  5.13 us
    pallas_call x1, Pallas kernels, mix(): pl.pallas_call(functools.partial(mix_kernel, seqs, width, local_heads), o...  4.88 us
  transfers between devices with their start and end apart: 16, of which 10 were waited for; matrix products, arithmetic and copies ran while one was open for 13% of the time, Pallas kernels for 30%

commit v1 on v0

--- a/solution.py
+++ b/solution.py
@@ -113,7 +113,6 @@
         out_specs=pl.BlockSpec(memory_space=VMEM),
         scratch_shapes=scratch,
         cost_estimate=cost(2),
-        name="project",
     )(*operands)
 
 
@@ -127,6 +126,13 @@
             distance * seqs : distance * seqs + count
         ]
     return silu(total)
+
+
+def as_column(row):
+    count = row.shape[1]
+    place = lax.broadcasted_iota(jnp.int32, (count, count), 0)
+    other = lax.broadcasted_iota(jnp.int32, (count, count), 1)
+    return jnp.sum(jnp.where(place == other, row, 0), axis=1, keepdims=True)
 
 
 def split(values):
@@ -153,7 +159,7 @@
     decay_ref,
 ):
     _, heads, head_dim, state_dim = state_ref.shape
-    seqs = accepted_ref.shape[0]
+    seqs = accepted_ref.shape[1]
     sequence = pl.program_id(0)
     count = path_x_ref.shape[0]
     group_width = HPG * head_dim
@@ -163,7 +169,7 @@
         lane = lax.broadcasted_iota(jnp.int32, (heads, heads * head_dim), 1)
         row = lax.broadcasted_iota(jnp.int32, (heads, heads * head_dim), 0)
         spread = jnp.where(lane // head_dim == row, 1.0, 0.0).astype(BF16)
-        accepted = accepted_ref[...]
+        accepted = as_column(accepted_ref[...])
         a_rate = -jnp.exp(a_log_ref[...])
         steps = softplus(path_dt_ref[...].astype(F32) + bias_ref[...])
         weights = []
@@ -240,7 +246,7 @@
     nodes = seqs * props
     parents = parents_ref[...]
     parent = jnp.concatenate([parents[:, place : place + 1] for place in range(props)], axis=0)
-    accepted = jnp.concatenate([accepted_ref[...]] * props, axis=0)
+    accepted = jnp.concatenate([as_column(accepted_ref[...])] * props, axis=0)
     row = lax.broadcasted_iota(jnp.int32, (nodes, nodes), 0)
     column = lax.broadcasted_iota(jnp.int32, (nodes, nodes), 1)
     own = lax.rem(lax.broadcasted_iota(jnp.int32, (nodes, 1), 0), seqs)
@@ -304,44 +310,53 @@
     )(parents, accepted, *inputs)
 
 
+def added(refs, span):
+    return sum(ref[:, span].astype(F32) for ref in refs)
+
+
 def mix_kernel(
     seqs,
     width,
     local_heads,
-    keep_bcr_ref,
-    got_bcr_ref,
-    keep_x_ref,
-    got_x_ref,
-    links_ref,
-    ancestry_ref,
-    before_ref,
-    taps_x_ref,
-    taps_b_ref,
-    taps_c_ref,
-    bias_ref,
-    rate_ref,
-    skip_ref,
-    state_ref,
-    out_ref,
-    scale_ref,
-    post_x_ref,
-    post_b_ref,
-    post_c_ref,
+    addends,
+    *refs,
 ):
-    nodes, inner = keep_x_ref.shape
+    bcr_refs = refs[:addends]
+    x_refs = refs[addends : 2 * addends]
+    (
+        links_ref,
+        ancestry_ref,
+        before_ref,
+        taps_x_ref,
+        taps_b_ref,
+        taps_c_ref,
+        bias_ref,
+        a_log_ref,
+        skip_ref,
+        state_ref,
+        out_ref,
+        scale_ref,
+        post_x_ref,
+        post_b_ref,
+        post_c_ref,
+    ) = refs[2 * addends :]
+    nodes, inner = x_refs[0].shape
     group_cols = taps_b_ref.shape[1]
     head_dim = inner // local_heads
     state_dim = state_ref.shape[3]
     groups = local_heads // HPG
     group_width = HPG * head_dim
     rate_start = 2 * group_cols
-    extra = keep_bcr_ref[:, rate_start:].astype(F32) + got_bcr_ref[:, rate_start:].astype(F32)
+    extra = added(bcr_refs, slice(rate_start, rate_start + LANES))
+    empty = jnp.zeros((1, LANES - local_heads), F32)
+    bias = jnp.concatenate([bias_ref[...], empty], axis=1)
+    a_rate = jnp.concatenate([-jnp.exp(a_log_ref[...]), empty], axis=1)
     scale = lax.rsqrt(extra[:, local_heads : local_heads + 1] / width + EPS)
     scale_ref[...] = jnp.broadcast_to(scale, scale_ref.shape)
 
     ancestry = ancestry_ref[...]
-    step = softplus((extra * scale).astype(BF16).astype(F32) + bias_ref[...])
-    decayed = step * rate_ref[...]
+    step = softplus((extra * scale).astype(BF16).astype(F32) + bias)
+    decayed = step * a_rate
     high, rest = split(decayed)
     middle, low = split(rest)
     parts = jnp.concatenate([high, middle, low], axis=1).astype(BF16)
@@ -352,12 +367,11 @@
     step_t = step.T
     is_live = ancestry > 0.5
 
-    def convolve(keep_ref, got_ref, taps_ref, source, start, target_ref):
+    def convolve(row_refs, taps_ref, source, start, target_ref):
         last = taps_ref.shape[0] - 1
         for lower in range(0, taps_ref.shape[1], CHUNK):
             span = slice(lower, lower + CHUNK)
-            taken = slice(source + lower, source + lower + CHUNK)
-            rows = keep_ref[:, taken].astype(F32) + got_ref[:, taken].astype(F32)
+            rows = added(row_refs, slice(source + lower, source + lower + CHUNK))
             rows = (rows * scale).astype(BF16)
             taps = taps_ref[:, span].astype(F32)
             found = dot(links_ref[...], rows)
@@ -369,9 +383,9 @@
                 ]
             target_ref[:, span] = silu(total).astype(target_ref.dtype)
 
-    convolve(keep_bcr_ref, got_bcr_ref, taps_b_ref, 0, inner, post_b_ref)
-    convolve(keep_bcr_ref, got_bcr_ref, taps_c_ref, group_cols, inner + group_cols, post_c_ref)
-    convolve(keep_x_ref, got_x_ref, taps_x_ref, 0, 0, post_x_ref)
+    convolve(bcr_refs, taps_b_ref, 0, inner, post_b_ref)
+    convolve(bcr_refs, taps_c_ref, group_cols, inner + group_cols, post_c_ref)
+    convolve(x_refs, taps_x_ref, 0, 0, post_x_ref)
 
     own = lax.rem(lax.broadcasted_iota(jnp.int32, (nodes, 1), 0), seqs)
     per_lanes = LANES // head_dim
@@ -422,80 +436,62 @@
             )
 
 
-def mix(
-    seqs,
-    width,
-    local_heads,
-    keep_bcr,
-    got_bcr,
-    keep_x,
-    got_x,
-    links,
-    ancestry,
-    before,
-    taps_x,
-    taps_b,
-    taps_c,
-    bias,
-    rate,
-    skip,
-    state,
-):
-    nodes, inner = keep_x.shape
-    operands = [
-        keep_bcr,
-        got_bcr,
-        keep_x,
-        got_x,
-        links,
-        ancestry,
-        before,
-        taps_x,
-        taps_b,
-        taps_c,
-        bias,
-        rate,
-        skip,
-        state,
+def first_rows(arrays, nodes):
+    return [pl.BlockSpec((nodes, array.shape[1]), lambda i: (0, 0)) for array in arrays]
+
+
+def full_blocks(arrays):
+    return [
+        pl.BlockSpec(array.shape, functools.partial(lambda rank, i: (0,) * rank, array.ndim))
+        for array in arrays
+    ]
+
+
+def mix(seqs, width, local_heads, bcr, x, others):
+    nodes, inner = x[-1].shape
+    group_cols = others[4].shape[1]
+    outs = [
+        jax.ShapeDtypeStruct((nodes, inner), F32),
+        jax.ShapeDtypeStruct((nodes, LANES), F32),
     ]
     return pl.pallas_call(
-        functools.partial(mix_kernel, seqs, width, local_heads),
-        out_shape=[
-            jax.ShapeDtypeStruct((nodes, inner), F32),
-            jax.ShapeDtypeStruct((nodes, LANES), F32),
-        ],
-        in_specs=whole(len(operands)),
-        out_specs=whole(2),
+        functools.partial(mix_kernel, seqs, width, local_heads, len(x)),
+        grid=(1,),
+        out_shape=outs,
+        in_specs=first_rows(bcr + x, nodes) + full_blocks(others),
+        out_specs=full_blocks(outs),
         scratch_shapes=[
             pltpu.VMEM((nodes, inner), F32),
-            pltpu.VMEM((nodes, taps_b.shape[1]), BF16),
-            pltpu.VMEM((nodes, taps_c.shape[1]), BF16),
+            pltpu.VMEM((nodes, group_cols), BF16),
+            pltpu.VMEM((nodes, group_cols), BF16),
         ],
         cost_estimate=cost(8),
         name="mix",
-    )(*operands)
-
-
-def gate_kernel(group_width, keep_ref, got_ref, scale_ref, heads_ref, gain_ref, out_ref):
+    )(*bcr, *x, *others)
+
+
+def gate_kernel(group_width, *refs):
+    *row_refs, scale_ref, heads_ref, gain_ref, out_ref = refs
     scale = scale_ref[:, :1]
     for lower in range(0, out_ref.shape[1], group_width):
         span = slice(lower, lower + group_width)
-        rows = keep_ref[:, span].astype(F32) + got_ref[:, span].astype(F32)
-        rows = (rows * scale).astype(BF16).astype(F32)
+        rows = (added(row_refs, span) * scale).astype(BF16).astype(F32)
         gated = heads_ref[:, span] * silu(rows)
         mean = jnp.sum(gated * gated, axis=1, keepdims=True) / group_width
         out_ref[:, span] = (gated * lax.rsqrt(mean + EPS) * gain_ref[:, span]).astype(BF16)
 
 
-def gate(group_width, keep, got, scale, heads_out, gain):
+def gate(group_width, rows, scale, heads_out, gain):
+    out = jax.ShapeDtypeStruct(heads_out.shape, BF16)
     return pl.pallas_call(
         functools.partial(gate_kernel, group_width),
-        out_shape=jax.ShapeDtypeStruct(heads_out.shape, BF16),
-        in_specs=whole(5),
-        out_specs=pl.BlockSpec(memory_space=VMEM),
+        grid=(1,),
+        out_shape=out,
+        in_specs=first_rows(rows, heads_out.shape[0]) + full_blocks([scale, heads_out, gain]),
+        out_specs=full_blocks([out])[0],
         cost_estimate=cost(1),
         name="gate",
-    )(keep, got, scale, heads_out, gain)
+    )(*rows, scale, heads_out, gain)
 
 
 def swap_bit(array, bit, blocks):
@@ -506,16 +502,11 @@
     return lax.optimization_barrier((value, *others))[0]
 
 
-def halving(keep, received, bit, blocks):
-    half = keep.shape[0] // 2
-    send = (keep[half:].astype(F32) + received[half:].astype(F32)).astype(BF16)
-
-    def stay(*others):
-        kept = after(keep, received, send, *others)
-        got = after(received, keep, send, *others)
-        return kept[:half].astype(F32) + got[:half].astype(F32)
-
-    return send, swap_bit(send, bit, blocks), stay
+def halving(addends, bit, blocks, *others):
+    half = addends[-1].shape[0] // 2
+    addends = [*addends[:-1], after(addends[-1], *others)]
+    send = sum(addend[half : 2 * half].astype(F32) for addend in addends).astype(BF16)
+    return send, [*addends, swap_bit(send, bit, blocks)]
 
 
 def mixer(
@@ -585,7 +576,7 @@
     keep_bcr = project(of_z[:half], after(tokens_q, send_z), *bcr_args)
     keep_x = project(of_x[:half], after(tokens_q, keep_bcr), *x_args)
 
-    accepted = accepted[:, None]
+    accepted = accepted[None, :]
     conv_x, conv_b, conv_c = by_position(conv_x), by_position(conv_b), by_position(conv_c)
     path_x, path_b, path_c = by_position(path_x), by_position(path_b), by_position(path_c)
     links, ancestry, before = tree(
@@ -593,12 +584,9 @@
         after(accepted, keep_x),
         [(conv_x, path_x, conv_wx), (conv_b, path_b, conv_wb), (conv_c, path_c, conv_wc)],
     )
-    sent_bcr, got_bcr, stay_bcr = halving(
-        keep_bcr, after(got_bcr, links), z_first[1], kv_count
-    )
-    sent_x, got_x, stay_x = halving(keep_x, after(got_x, sent_bcr), x_first[1], kv_count)
+    sent_bcr, bcr = halving([keep_bcr, got_bcr], z_first[1], kv_count, links)
+    sent_x, x = halving([keep_x, got_x], x_first[1], kv_count, sent_bcr)
     keep_z = project(of_x[:half], after(tokens_q, sent_x), *z_args)
-    a_rate = -jnp.exp(a_log)
     new_state, half_state = replay_state(
         after(accepted, keep_z),
         by_position(path_dt),
@@ -612,51 +600,32 @@
         conv_wb,
         state,
     )
-    keep_bcr = stay_bcr(keep_z)
-    keep_x = stay_x(keep_z)
-    sent_z, got_z, stay_z = halving(
-        keep_z, after(got_z, half_state, keep_bcr, keep_x), x_first[1], kv_count
-    )
+    sent_z, z = halving([keep_z, got_z], x_first[1], kv_count, half_state)
     for place in range(2, len(x_first)):
-        sent_x, got_x, stay_x = halving(
-            keep_x, after(got_x, sent_z), x_first[place], kv_count
-        )
-        sent_bcr, got_bcr, stay_bcr = halving(
-            keep_bcr, after(got_bcr, sent_x), z_first[place], kv_count
-        )
-        keep_x = stay_x(sent_bcr)
-        keep_bcr = stay_bcr(sent_bcr)
-        keep_z = stay_z(sent_bcr)
-        sent_z, got_z, stay_z = halving(
-            keep_z, after(got_z, keep_x, keep_bcr), x_first[place], kv_count
-        )
-    got_x = after(got_x, sent_z)
-    got_bcr = after(got_bcr, sent_z)
-    keep_z = stay_z(sent_z)
-
-    def padded(values):
-        return jnp.pad(values, (0, LANES - heads_local))[None, :]
+        sent_x, x = halving(x, x_first[place], kv_count, sent_z)
+        sent_bcr, bcr = halving(bcr, z_first[place], kv_count, sent_x)
+        sent_z, z = halving(z, x_first[place], kv_count, sent_bcr)
 
     heads_out, row_scale = mix(
         seq_local,
         width,
         heads_local,
-        keep_bcr,
-        got_bcr,
-        keep_x,
-        got_x,
-        links,
-        ancestry,
-        before,
-        conv_wx,
-        conv_wb,
-        conv_wc,
-        padded(dt_bias),
-        padded(a_rate),
-        d_skip[None, :],
-        half_state,
+        [*bcr[:-1], after(bcr[-1], sent_z)],
+        [*x[:-1], after(x[-1], sent_z)],
+        [
+            links,
+            ancestry,
+            before,
+            conv_wx,
+            conv_wb,
+            conv_wc,
+            dt_bias[None, :],
+            a_log[None, :],
+            d_skip[None, :],
+            half_state,
+        ],
     )
-    gated = gate(HPG * head_dim, keep_z, got_z, row_scale, heads_out, gain_out[None, :])
+    gated = gate(HPG * head_dim, z, row_scale, heads_out, gain_out[None, :])
 
     w_out = after(w_out, sent_bcr, sent_x)
     w_pieces = [w_out]

time: 114 us -> 121 us (1.061)
  the two profiles are of different devices: /device:TPU:4 before, /device:TPU:0 now
where the time goes in v1:
time: 121 us; the launch traced here: 119 us
  waiting for transfers between devices  46.1 us (38%)
  Pallas kernels  38.5 us (32%)
  starting transfers between devices  20.2 us (17%)
  other arithmetic  9.81 us (8%)
  matrix products  1.89 us (2%)
  local copies, waits for them, and re-layouts  1.42 us (1%)
    ppermute x13, waiting for transfers between devices, swap_bit(): return lax.ppermute(array, 'kv', [(i, i ^ 1 << bit) for i in range(blocks)])  39.2 us
    pallas_call x6, Pallas kernels, project(): pl.pallas_call(functools.partial(project_kernel, tuple(differences), w_dt...  18.9 us
    ppermute x13, starting transfers between devices, swap_bit(): return lax.ppermute(array, 'kv', [(i, i ^ 1 << bit) for i in range(blocks)])  14.3 us
    pallas_call x1, Pallas kernels, replay_state(): pl.pallas_call(state_kernel, grid=(seqs,), out_shape=[jax.ShapeDtypeStruc...  8.61 us
    convert_element_type x6, other arithmetic, halving(): sum((addend[half:2 * half].astype(F32) for addend in addends)).astype(BF16)  7.56 us
    ppermute x2, starting transfers between devices, mixer(): total = total + lax.ppermute(piece, ('kv', 'tp'), route).astype(F32)  5.84 us
    ppermute x2, waiting for transfers between devices, mixer(): total = total + lax.ppermute(piece, ('kv', 'tp'), route).astype(F32)  5.28 us
    pallas_call x1, Pallas kernels, mix(): pl.pallas_call(functools.partial(mix_kernel, seqs, width, local_heads, le...  5.12 us
  transfers between devices with their start and end apart: 16, of which 10 were waited for; matrix products, arithmetic and copies ran while one was open for 8% of the time, Pallas kernels for 29%

profile of v1, /device:TPU:0, one launch (start us, length us, event | category | flops | bytes accessed | tf_op | source)
XLA Modules:
  0.0 118.7 jit_solution(15248940451896150846)
XLA Ops:
  0.6 3.5 %shard_map.248 = bf16[384,1152]{1,0:T(8,128)(2,1)} custom-call(bf16[12,8,8,512]{3,2,1,0:T(8,128)(2,1)} %bitcast.44, f32[1,4096]{1,0:T(1,128)} %bitcast.53, bf16[64,4096]{1,0:T(8,128)(2,1)} %bitcast.50, bf16[512,512]{1,0:T(8,128)(2,1)} %refs_1_.3, bf16[512,512]{1,0:T(8,128)(2,1)} %refs_2_.4), custom_call_target="tpu_custom_call" | custom-call | flops 8000000 | bytes 1024 | tf_op jit(solution)/shard_map/pallas_call | solution.py:109
  4.1 3.1 %collective-permute-start.1 = (bf16[384,1152]{1,0:T(8,128)(2,1)}, bf16[384,1152]{1,0:T(8,128)(2,1)S(1)}, u32[]{:S(2)}, u32[]{:S(2)}) collective-permute-start(bf16[384,1152]{1,0:T(8,128)(2,1)} %shard_map.248), channel_id=1, source_target_pairs={{0,8},{4,12},{8,0},{12,4},{16,24},{20,28},{24,16},{28,20},{1,9},{5... | collective-permute-start | bytes 2654216 | tf_op jit(solution)/shard_map/ppermute | solution.py:498
  7.2 3.0 %shard_map.249 = bf16[384,1024]{1,0:T(8,128)(2,1)} custom-call(bf16[12,8,8,512]{3,2,1,0:T(8,128)(2,1)} %bitcast.45, f32[1,4096]{1,0:T(1,128)} %bitcast.54, bf16[512,1024]{1,0:T(8,128)(2,1)} %refs_0_.6), custom_call_target="tpu_custom_call" | custom-call | flops 8000000 | bytes 1024 | tf_op jit(solution)/shard_map/pallas_call | solution.py:109
  10.1 1.5 %collective-permute-start = (bf16[384,1024]{1,0:T(8,128)(2,1)}, bf16[384,1024]{1,0:T(8,128)(2,1)S(1)}, u32[]{:S(2)}, u32[]{:S(2)}) collective-permute-start(bf16[384,1024]{1,0:T(8,128)(2,1)} %shard_map.249), channel_id=1, source_target_pairs={{0,4},{4,0},{8,12},{12,8},{16,20},{20,16},{24,28},{28,24},{1,5},{5... | collective-permute-start | bytes 2359304 | tf_op jit(solution)/shard_map/ppermute | solution.py:498
  11.6 3.0 %shard_map.250 = bf16[384,1024]{1,0:T(8,128)(2,1)} custom-call(bf16[12,8,8,512]{3,2,1,0:T(8,128)(2,1)} %bitcast.46, f32[1,4096]{1,0:T(1,128)} %bitcast.55, bf16[512,1024]{1,0:T(8,128)(2,1)} %refs_0_.7), custom_call_target="tpu_custom_call" | custom-call | flops 8000000 | bytes 1024 | tf_op jit(solution)/shard_map/pallas_call | solution.py:109
  15.2 3.5 %shard_map.251.refs_0_ = bf16[384,1152]{1,0:T(8,128)(2,1)} custom-call(bf16[12,8,8,512]{3,2,1,0:T(8,128)(2,1)} %bitcast.47, f32[1,4096]{1,0:T(1,128)} %bitcast.56, bf16[64,4096]{1,0:T(8,128)(2,1)} %bitcast.51, bf16[512,512]{1,0:T(8,128)(2,1)} %refs_1_.3, bf16[512,512]{1,0:T(8,128)(2,1)} %refs_2_.4), custom_call_target="tpu_custom_call" | custom-call | flops 8000000 | bytes 1024 | tf_op jit(solution)/shard_map/pallas_call | solution.py:109
  18.7 3.0 %shard_map.252.refs_4_ = bf16[384,1024]{1,0:T(8,128)(2,1)} custom-call(bf16[12,8,8,512]{3,2,1,0:T(8,128)(2,1)} %bitcast.48, f32[1,4096]{1,0:T(1,128)} %bitcast.57, bf16[512,1024]{1,0:T(8,128)(2,1)} %refs_0_.6), custom_call_target="tpu_custom_call" | custom-call | flops 8000000 | bytes 1024 | tf_op jit(solution)/shard_map/pallas_call | solution.py:109
  21.7 3.4 %tree.1 = (bf16[288,96]{1,0:T(8,128)(2,1)}, f32[96,96]{1,0:T(8,128)}, f32[96,2048]{1,0:T(8,128)}) custom-call(s32[8,12]{1,0:T(8,128)} %parents_ref.1, s32[1,8]{1,0:T(1,128)} %bitcast.71, bf16[24,1024]{1,0:T(8,128)(2,1)} %bitcast.61, bf16[48,1024]{1,0:T(8,128)(2,1)} %bitcast.59, bf16[4,1024]{1,0:T(4,128)(2,1)} %refs_11_.1, bf16[24,512]{1,0:T(8,128)(2,1)} %bitcast.65, ...), custom_call_target="tpu_custom_call" | custom-call | flops 16000000 | bytes 1024 | tf_op jit(solution)/shard_map/tree/pallas_call | solution.py:299
  25.1 1.9 %collective-permute-done.1.refs_1_ = bf16[384,1152]{1,0:T(8,128)(2,1)S(1)} collective-permute-done((bf16[384,1152]{1,0:T(8,128)(2,1)}, bf16[384,1152]{1,0:T(8,128)(2,1)S(1)}, u32[]{:S(2)}, u32[]{:S(2)}) %collective-permute-start.1) | collective-permute-done | bytes 884768 | tf_op jit(solution)/shard_map/ppermute | solution.py:498
  28.0 2.7 %collective-permute-done.refs_5_ = bf16[384,1024]{1,0:T(8,128)(2,1)S(1)} collective-permute-done((bf16[384,1024]{1,0:T(8,128)(2,1)}, bf16[384,1024]{1,0:T(8,128)(2,1)S(1)}, u32[]{:S(2)}, u32[]{:S(2)}) %collective-permute-start) | collective-permute-done | bytes 786464 | tf_op jit(solution)/shard_map/ppermute | solution.py:498
  30.8 2.2 %add_convert_fusion.3 = bf16[192,1024]{1,0:T(8,128)(2,1)} fusion(bf16[384,1024]{1,0:T(8,128)(2,1)} %shard_map.252.refs_4_, bf16[384,1024]{1,0:T(8,128)(2,1)S(1)} %collective-permute-done.refs_5_), kind=kLoop, calls=%fused_computation.10 | loop fusion | flops 786432 | bytes 1179648 | tf_op jit(solution)/shard_map/convert_element_type | solution.py:508
  32.9 3.0 %collective-permute-start.4 = (bf16[192,1152]{1,0:T(8,128)(2,1)}, bf16[192,1152]{1,0:T(8,128)(2,1)}, u32[]{:S(2)}, u32[]{:S(2)}) collective-permute-start(bf16[192,1152]{1,0:T(8,128)(2,1)} %add_convert_fusion), channel_id=1, source_target_pairs={{0,16},{4,20},{8,24},{12,28},{16,0},{20,4},{24,8},{28,12},{1,17},{... | collective-permute-start | bytes 1327112 | tf_op jit(solution)/shard_map/ppermute | solution.py:498
  36.0 3.0 %shard_map.253.refs_0_ = bf16[384,1024]{1,0:T(8,128)(2,1)} custom-call(bf16[12,8,8,512]{3,2,1,0:T(8,128)(2,1)} %bitcast.49, f32[1,4096]{1,0:T(1,128)} %bitcast.58, bf16[512,1024]{1,0:T(8,128)(2,1)} %refs_0_.7), custom_call_target="tpu_custom_call" | custom-call | flops 8000000 | bytes 1024 | tf_op jit(solution)/shard_map/pallas_call | solution.py:109
  39.0 8.6 %replay_state.1 = (f32[8,16,64,128]{3,2,1,0:T(8,128)}, bf16[8,16,64,128]{3,2,1,0:T(8,128)(2,1)}) custom-call(s32[1,8]{1,0:T(1,128)} %bitcast.72, bf16[48,16]{1,0:T(8,128)(2,1)} %bitcast.69, f32[1,16]{1,0:T(1,128)} %bitcast.73, f32[1,16]{1,0:T(1,128)} %bitcast.75, bf16[24,1024]{1,0:T(8,128)(2,1)} %bitcast.62, bf16[48,1024]{1,0:T(8,128)(2,1)} %bitcast.60, ...), custom_call_target="tpu_custom_call" | custom-call | flops 32000000 | bytes 1024 | tf_op jit(solution)/shard_map/replay_state/pallas_call | solution.py:224
  47.6 1.1 add_convert_fusion.2
  48.7 2.0 %collective-permute-done.5.refs_6_ = bf16[192,1024]{1,0:T(8,128)(2,1)} collective-permute-done((bf16[192,1024]{1,0:T(8,128)(2,1)}, bf16[192,1024]{1,0:T(8,128)(2,1)}, u32[]{:S(2)}, u32[]{:S(2)}) %collective-permute-start.5) | collective-permute-done | bytes 393248 | tf_op jit(solution)/shard_map/ppermute | solution.py:498
  50.8 1.1 add_convert_fusion.7
  51.9 1.6 %collective-permute-done.4.refs_2_ = bf16[192,1152]{1,0:T(8,128)(2,1)} collective-permute-done((bf16[192,1152]{1,0:T(8,128)(2,1)}, bf16[192,1152]{1,0:T(8,128)(2,1)}, u32[]{:S(2)}, u32[]{:S(2)}) %collective-permute-start.4) | collective-permute-done | bytes 442400 | tf_op jit(solution)/shard_map/ppermute | solution.py:498
  53.5 1.0 add_convert_fusion.4
  54.5 1.6 %collective-permute-start.10 = (bf16[1024,512]{1,0:T(8,128)(2,1)}, bf16[1024,512]{1,0:T(8,128)(2,1)S(1)}, u32[]{:S(2)}, u32[]{:S(2)}) collective-permute-start(bf16[1024,512]{1,0:T(8,128)(2,1)} %param.49), channel_id=1, source_target_pairs={{0,4},{4,0},{8,12},{12,8},{16,20},{20,16},{24,28},{28,24},{1,5},{5... | collective-permute-start | bytes 3145736 | tf_op jit(solution)/shard_map/ppermute | solution.py:498
  56.6 3.4 %collective-permute-start.8 = (bf16[96,1024]{1,0:T(8,128)(2,1)S(1)}, bf16[96,1024]{1,0:T(8,128)(2,1)S(1)}, u32[]{:S(2)}, u32[]{:S(2)}) collective-permute-start(bf16[96,1024]{1,0:T(8,128)(2,1)S(1)} %add_convert_fusion.7), channel_id=1, source_target_pairs={{0,16},{4,20},{8,24},{12,28},{16,0},{20,4},{24,8},{28,12},{1,17},{... | collective-permute-start | bytes 589832 | tf_op jit(solution)/shard_map/ppermute | solution.py:498
  60.6 7.5 %collective-permute-done.3.refs_2_ = bf16[192,1024]{1,0:T(8,128)(2,1)S(1)} collective-permute-done((bf16[192,1024]{1,0:T(8,128)(2,1)S(1)}, bf16[192,1024]{1,0:T(8,128)(2,1)S(1)}, u32[]{:S(2)}, u32[]{:S(2)}) %collective-permute-start.3) | collective-permute-done | bytes 393248 | tf_op jit(solution)/shard_map/ppermute | solution.py:498
  68.1 1.1 add_convert_fusion.6
  69.4 12.3 %collective-permute-done.7.refs_3_ = bf16[96,1152]{1,0:T(8,128)(2,1)S(1)} collective-permute-done((bf16[96,1152]{1,0:T(8,128)(2,1)S(1)}, bf16[96,1152]{1,0:T(8,128)(2,1)S(1)}, u32[]{:S(2)}, u32[]{:S(2)}) %collective-permute-start.7) | collective-permute-done | bytes 221216 | tf_op jit(solution)/shard_map/ppermute | solution.py:498
  82.4 5.1 %mix.1 = (f32[96,1024]{1,0:T(8,128)}, f32[96,128]{1,0:T(8,128)}) custom-call(bf16[384,1152]{1,0:T(8,128)(2,1)} %shard_map.251.refs_0_, bf16[384,1152]{1,0:T(8,128)(2,1)} %copy-done.2, bf16[192,1152]{1,0:T(8,128)(2,1)} %collective-permute-done.4.refs_2_, bf16[96,1152]{1,0:T(8,128)(2,1)} %copy-done.5, bf16[384,1024]{1,0:T(8,128)(2,1)} %shard_map.252.refs_4_, ...), custom_call_target="tpu_custom_call" | custom-call | flops 32000000 | bytes 1024 | tf_op jit(solution)/shard_map/mix/pallas_call | solution.py:457
  88.2 2.3 %gate.1 = bf16[96,1024]{1,0:T(8,128)(2,1)} custom-call(bf16[384,1024]{1,0:T(8,128)(2,1)} %shard_map.253.refs_0_, bf16[384,1024]{1,0:T(8,128)(2,1)} %collective-permute-done.2.refs_1_, bf16[192,1024]{1,0:T(8,128)(2,1)} %copy-done.4, bf16[96,1024]{1,0:T(8,128)(2,1)} %copy-done.8, f32[96,128]{1,0:T(8,128)} %get-tuple-element.46.refs_4_, ...), custom_call_target="tpu_custom_call" | custom-call | flops 4000000 | bytes 1024 | tf_op jit(solution)/shard_map/gate/pallas_call | solution.py:486
  90.5 8.2 %collective-permute-done.11 = bf16[96,1024]{1,0:T(8,128)(2,1)S(1)} collective-permute-done((bf16[96,1024]{1,0:T(8,128)(2,1)}, bf16[96,1024]{1,0:T(8,128)(2,1)S(1)}, u32[]{:S(2)}, u32[]{:S(2)}) %collective-permute-start.11) | collective-permute-done | bytes 196640 | tf_op jit(solution)/shard_map/ppermute | solution.py:498
  98.7 1.4 %broadcast_select_fusion.1 = (bf16[1024,512]{1,0:T(8,128)(2,1)S(1)}, bf16[1024,512]{1,0:T(8,128)(2,1)S(1)}) fusion(bf16[1024,512]{1,0:T(8,128)(2,1)S(1)} %collective-permute-done.10, bf16[1024,512]{1,0:T(8,128)(2,1)} %param.49, pred[]{:T(512)S(6)} %eq.7), kind=kLoop, calls=%fused_computation.6 | loop fusion | flops 1048576 | bytes 4194305 | tf_op jit(solution)/shard_map/jit(_where)/select_n | solution.py:638
  101.6 2.8 %collective-permute-done.12 = bf16[96,1024]{1,0:T(8,128)(2,1)S(1)} collective-permute-done((bf16[96,1024]{1,0:T(8,128)(2,1)S(1)}, bf16[96,1024]{1,0:T(8,128)(2,1)S(1)}, u32[]{:S(2)}, u32[]{:S(2)}) %collective-permute-start.12) | collective-permute-done | bytes 196640 | tf_op jit(solution)/shard_map/ppermute | solution.py:498
  105.0 1.7 %collective-permute-done.13 = bf16[192,1024]{1,0:T(8,128)(2,1)S(1)} collective-permute-done((bf16[192,1024]{1,0:T(8,128)(2,1)S(1)}, bf16[192,1024]{1,0:T(8,128)(2,1)S(1)}, u32[]{:S(2)}, u32[]{:S(2)}) %collective-permute-start.13) | collective-permute-done | bytes 393248 | tf_op jit(solution)/shard_map/ppermute | solution.py:654
  107.6 5.2 %collective-permute-start.15 = (bf16[96,1024]{1,0:T(8,128)(2,1)S(1)}, bf16[96,1024]{1,0:T(8,128)(2,1)S(1)}, u32[]{:S(2)}, u32[]{:S(2)}) collective-permute-start(bf16[96,1024]{1,0:T(8,128)(2,1)S(1)} %get-tuple-element.55), channel_id=1, source_target_pairs={{0,16},{1,24},{2,0},{3,8},{4,20},{5,28},{6,4},{7,12},{8,17},{9,25}... | collective-permute-start | bytes 589832 | tf_op jit(solution)/shard_map/ppermute | solution.py:673
  112.7 5.3 %collective-permute-done.15 = bf16[96,1024]{1,0:T(8,128)(2,1)S(1)} collective-permute-done((bf16[96,1024]{1,0:T(8,128)(2,1)S(1)}, bf16[96,1024]{1,0:T(8,128)(2,1)S(1)}, u32[]{:S(2)}, u32[]{:S(2)}) %collective-permute-start.15) | collective-permute-done | bytes 196640 | tf_op jit(solution)/shard_map/ppermute | solution.py:673
  (43 shorter events, 7.7 us)
Async XLA Ops:
  4.1 22.9 %collective-permute-start.1 = (bf16[384,1152]{1,0:T(8,128)(2,1)}, bf16[384,1152]{1,0:T(8,128)(2,1)S(1)}, u32[]{:S(2)}, u32[]{:S(2)}) collective-permute-start(bf16[384,1152]{1,0:T(8,128)(2,1)} %shard_map.248), channel_id=1, source_target_pairs={{0,8},{4,12},{8,0},{12,4},{16,24},{20,28},{24,16},{28,20},{1,9},{5... | collective-permute-start | bytes 2654216 | tf_op jit(solution)/shard_map/ppermute | solution.py:498
  10.1 20.6 %collective-permute-start = (bf16[384,1024]{1,0:T(8,128)(2,1)}, bf16[384,1024]{1,0:T(8,128)(2,1)S(1)}, u32[]{:S(2)}, u32[]{:S(2)}) collective-permute-start(bf16[384,1024]{1,0:T(8,128)(2,1)} %shard_map.249), channel_id=1, source_target_pairs={{0,4},{4,0},{8,12},{12,8},{16,20},{20,16},{24,28},{28,24},{1,5},{5... | collective-permute-start | bytes 2359304 | tf_op jit(solution)/shard_map/ppermute | solution.py:498
  14.6 32.9 %collective-permute-start.2 = (bf16[384,1024]{1,0:T(8,128)(2,1)}, bf16[384,1024]{1,0:T(8,128)(2,1)}, u32[]{:S(2)}, u32[]{:S(2)}) collective-permute-start(bf16[384,1024]{1,0:T(8,128)(2,1)} %shard_map.250), channel_id=1, source_target_pairs={{0,4},{4,0},{8,12},{12,8},{16,20},{20,16},{24,28},{28,24},{1,5},{5... | collective-permute-start | bytes 2359304 | tf_op jit(solution)/shard_map/ppermute | solution.py:498
  18.7 8.4 %copy-start = (bf16[384,1152]{1,0:T(8,128)(2,1)S(1)}, bf16[384,1152]{1,0:T(8,128)(2,1)}, u32[]{:S(2)}) copy-start(bf16[384,1152]{1,0:T(8,128)(2,1)} %shard_map.251.refs_0_) | copy-start | bytes 2654212
  27.0 26.4 %copy-start.2 = (bf16[384,1152]{1,0:T(8,128)(2,1)}, bf16[384,1152]{1,0:T(8,128)(2,1)S(1)}, u32[]{:S(2)}) copy-start(bf16[384,1152]{1,0:T(8,128)(2,1)S(1)} %collective-permute-done.1.refs_1_) | copy-start | bytes 2654212
  30.8 20.0 %copy-start.3 = (bf16[384,1024]{1,0:T(8,128)(2,1)}, bf16[384,1024]{1,0:T(8,128)(2,1)S(1)}, u32[]{:S(2)}) copy-start(bf16[384,1024]{1,0:T(8,128)(2,1)S(1)} %collective-permute-done.refs_5_) | copy-start | bytes 2359300
  32.9 17.8 %collective-permute-start.5 = (bf16[192,1024]{1,0:T(8,128)(2,1)}, bf16[192,1024]{1,0:T(8,128)(2,1)}, u32[]{:S(2)}, u32[]{:S(2)}) collective-permute-start(bf16[192,1024]{1,0:T(8,128)(2,1)} %add_convert_fusion.3), channel_id=1, source_target_pairs={{0,8},{4,12},{8,0},{12,4},{16,24},{20,28},{24,16},{28,20},{1,9},{5... | collective-permute-start | bytes 1179656 | tf_op jit(solution)/shard_map/ppermute | solution.py:498
  32.9 20.5 %collective-permute-start.4 = (bf16[192,1152]{1,0:T(8,128)(2,1)}, bf16[192,1152]{1,0:T(8,128)(2,1)}, u32[]{:S(2)}, u32[]{:S(2)}) collective-permute-start(bf16[192,1152]{1,0:T(8,128)(2,1)} %add_convert_fusion), channel_id=1, source_target_pairs={{0,16},{4,20},{8,24},{12,28},{16,0},{20,4},{24,8},{28,12},{1,17},{... | collective-permute-start | bytes 1327112 | tf_op jit(solution)/shard_map/ppermute | solution.py:498
  38.9 8.6 %copy-start.1 = (bf16[384,1024]{1,0:T(8,128)(2,1)S(1)}, bf16[384,1024]{1,0:T(8,128)(2,1)}, u32[]{:S(2)}) copy-start(bf16[384,1024]{1,0:T(8,128)(2,1)} %shard_map.253.refs_0_) | copy-start | bytes 2359300
  54.5 44.2 %collective-permute-start.10 = (bf16[1024,512]{1,0:T(8,128)(2,1)}, bf16[1024,512]{1,0:T(8,128)(2,1)S(1)}, u32[]{:S(2)}, u32[]{:S(2)}) collective-permute-start(bf16[1024,512]{1,0:T(8,128)(2,1)} %param.49), channel_id=1, source_target_pairs={{0,4},{4,0},{8,12},{12,8},{16,20},{20,16},{24,28},{28,24},{1,5},{5... | collective-permute-start | bytes 3145736 | tf_op jit(solution)/shard_map/ppermute | solution.py:498
  56.1 12.0 %collective-permute-start.3 = (bf16[192,1024]{1,0:T(8,128)(2,1)S(1)}, bf16[192,1024]{1,0:T(8,128)(2,1)S(1)}, u32[]{:S(2)}, u32[]{:S(2)}) collective-permute-start(bf16[192,1024]{1,0:T(8,128)(2,1)S(1)} %add_convert_fusion.2), channel_id=1, source_target_pairs={{0,8},{4,12},{8,0},{12,4},{16,24},{20,28},{24,16},{28,20},{1,9},{5... | collective-permute-start | bytes 1179656 | tf_op jit(solution)/shard_map/ppermute | solution.py:498
  56.6 12.7 %collective-permute-start.8 = (bf16[96,1024]{1,0:T(8,128)(2,1)S(1)}, bf16[96,1024]{1,0:T(8,128)(2,1)S(1)}, u32[]{:S(2)}, u32[]{:S(2)}) collective-permute-start(bf16[96,1024]{1,0:T(8,128)(2,1)S(1)} %add_convert_fusion.7), channel_id=1, source_target_pairs={{0,16},{4,20},{8,24},{12,28},{16,0},{20,4},{24,8},{28,12},{1,17},{... | collective-permute-start | bytes 589832 | tf_op jit(solution)/shard_map/ppermute | solution.py:498
  60.1 21.6 %collective-permute-start.7 = (bf16[96,1152]{1,0:T(8,128)(2,1)S(1)}, bf16[96,1152]{1,0:T(8,128)(2,1)S(1)}, u32[]{:S(2)}, u32[]{:S(2)}) collective-permute-start(bf16[96,1152]{1,0:T(8,128)(2,1)S(1)} %add_convert_fusion.4), channel_id=1, source_target_pairs={{0,4},{4,0},{8,12},{12,8},{16,20},{20,16},{24,28},{28,24},{1,5},{5... | collective-permute-start | bytes 663560 | tf_op jit(solution)/shard_map/ppermute | solution.py:498
  68.1 19.4 %copy-start.4 = (bf16[192,1024]{1,0:T(8,128)(2,1)}, bf16[192,1024]{1,0:T(8,128)(2,1)S(1)}, u32[]{:S(2)}) copy-start(bf16[192,1024]{1,0:T(8,128)(2,1)S(1)} %collective-permute-done.3.refs_2_) | copy-start | bytes 1179652
  69.2 18.2 %collective-permute-start.6 = (bf16[96,1024]{1,0:T(8,128)(2,1)S(1)}, bf16[96,1024]{1,0:T(8,128)(2,1)S(1)}, u32[]{:S(2)}, u32[]{:S(2)}) collective-permute-start(bf16[96,1024]{1,0:T(8,128)(2,1)S(1)} %add_convert_fusion.6), channel_id=1, source_target_pairs={{0,16},{4,20},{8,24},{12,28},{16,0},{20,4},{24,8},{28,12},{1,17},{... | collective-permute-start | bytes 589832 | tf_op jit(solution)/shard_map/ppermute | solution.py:498
  69.3 12.3 %copy-start.7 = (bf16[96,1024]{1,0:T(8,128)(2,1)}, bf16[96,1024]{1,0:T(8,128)(2,1)S(1)}, u32[]{:S(2)}) copy-start(bf16[96,1024]{1,0:T(8,128)(2,1)S(1)} %collective-permute-done.8.refs_7_) | copy-start | bytes 589828
  81.7 0.7 copy-start.5
  87.5 0.7 copy-start.8
  90.5 8.2 %collective-permute-start.11 = (bf16[96,1024]{1,0:T(8,128)(2,1)}, bf16[96,1024]{1,0:T(8,128)(2,1)S(1)}, u32[]{:S(2)}, u32[]{:S(2)}) collective-permute-start(bf16[96,1024]{1,0:T(8,128)(2,1)} %gate.1), channel_id=1, source_target_pairs={{0,16},{4,20},{8,24},{12,28},{16,0},{20,4},{24,8},{28,12},{1,17},{... | collective-permute-start | bytes 589832 | tf_op jit(solution)/shard_map/ppermute | solution.py:498
  90.5 9.6 %copy-start.6 = (bf16[96,1024]{1,0:T(8,128)(2,1)S(1)}, bf16[96,1024]{1,0:T(8,128)(2,1)}, u32[]{:S(2)}) copy-start(bf16[96,1024]{1,0:T(8,128)(2,1)} %gate.1) | copy-start | bytes 589828
  90.5 10.1 %collective-permute-start.9 = (bf16[96,1024]{1,0:T(8,128)(2,1)}, bf16[96,1024]{1,0:T(8,128)(2,1)S(1)}, u32[]{:S(2)}, u32[]{:S(2)}) collective-permute-start(bf16[96,1024]{1,0:T(8,128)(2,1)} %gate.1), channel_id=1, source_target_pairs={{0,8},{4,12},{8,0},{12,4},{16,24},{20,28},{24,16},{28,20},{1,9},{5... | collective-permute-start | bytes 589832 | tf_op jit(solution)/shard_map/ppermute | solution.py:498
  98.7 5.7 %collective-permute-start.12 = (bf16[96,1024]{1,0:T(8,128)(2,1)S(1)}, bf16[96,1024]{1,0:T(8,128)(2,1)S(1)}, u32[]{:S(2)}, u32[]{:S(2)}) collective-permute-start(bf16[96,1024]{1,0:T(8,128)(2,1)S(1)} %collective-permute-done.11), channel_id=1, source_target_pairs={{0,8},{4,12},{8,0},{12,4},{16,24},{20,28},{24,16},{28,20},{1,9},{5... | collective-permute-start | bytes 589832 | tf_op jit(solution)/shard_map/ppermute | solution.py:498
  104.9 1.8 %collective-permute-start.13 = (bf16[192,1024]{1,0:T(8,128)(2,1)S(1)}, bf16[192,1024]{1,0:T(8,128)(2,1)S(1)}, u32[]{:S(2)}, u32[]{:S(2)}) collective-permute-start(bf16[192,1024]{1,0:T(8,128)(2,1)S(1)} %pad_maximum_fusion.1), channel_id=1, source_target_pairs={{0,1},{1,0},{2,3},{3,2},{4,5},{5,4},{6,7},{7,6},{8,9},{9,8},{10,11... | collective-permute-start | bytes 1179656 | tf_op jit(solution)/shard_map/ppermute | solution.py:654
  106.9 5.9 %collective-permute-start.14 = (bf16[96,1024]{1,0:T(8,128)(2,1)S(1)}, bf16[96,1024]{1,0:T(8,128)(2,1)S(1)}, u32[]{:S(2)}, u32[]{:S(2)}) collective-permute-start(bf16[96,1024]{1,0:T(8,128)(2,1)S(1)} %get-tuple-element.54), channel_id=1, source_target_pairs={{0,0},{1,8},{2,16},{3,24},{4,4},{5,12},{6,20},{7,28},{8,1},{9,9},{... | collective-permute-start | bytes 589832 | tf_op jit(solution)/shard_map/ppermute | solution.py:673
  107.6 10.4 %collective-permute-start.15 = (bf16[96,1024]{1,0:T(8,128)(2,1)S(1)}, bf16[96,1024]{1,0:T(8,128)(2,1)S(1)}, u32[]{:S(2)}, u32[]{:S(2)}) collective-permute-start(bf16[96,1024]{1,0:T(8,128)(2,1)S(1)} %get-tuple-element.55), channel_id=1, source_target_pairs={{0,16},{1,24},{2,0},{3,8},{4,20},{5,28},{6,4},{7,12},{8,17},{9,25}... | collective-permute-start | bytes 589832 | tf_op jit(solution)/shard_map/ppermute | solution.py:673

commit v2 on v1

--- a/solution.py
+++ b/solution.py
@@ -12,6 +12,7 @@
 EPS = 1e-06
 LANES = 128
 CHUNK = 256
+RATE_ROWS = 32
 VMEM = pltpu.VMEM
 F32 = jnp.float32
 BF16 = jnp.bfloat16
@@ -60,7 +61,7 @@
     me = lax.axis_index("kv")
     rows_local = props * seqs
     if with_rate:
-        w_dt_ref, *w_refs, out_ref, scaled_ref, squares_ref = refs
+        w_dt_ref, *w_refs, out_ref, rate_ref, scaled_ref, squares_ref = refs
     else:
         *w_refs, out_ref, scaled_ref = refs
     slab_start = pl.multiple_of(me * width, LANES)
@@ -70,7 +71,9 @@
         span = slice(position * rows_local, (position + 1) * rows_local)
         scaled_ref[span] = (rows * gain).astype(BF16)
         if with_rate:
-            squares_ref[span] = jnp.sum(rows * rows, axis=1, keepdims=True)
+            high, low = split(rows * rows)
+            squares_ref[0, span] = high.astype(BF16)
+            squares_ref[1, span] = low.astype(BF16)
     start = 0
     for w_ref in w_refs:
         for lower in range(0, w_ref.shape[1], CHUNK):
@@ -83,34 +86,35 @@
         heads = w_dt_ref.shape[0]
         local = heads // tp_count
         first = lax.axis_index("tp") * local
-        row = lax.broadcasted_iota(jnp.int32, (LANES, heads), 0)
-        column = lax.broadcasted_iota(jnp.int32, (LANES, heads), 1)
+        row = lax.broadcasted_iota(jnp.int32, (RATE_ROWS, heads), 0)
+        column = lax.broadcasted_iota(jnp.int32, (RATE_ROWS, heads), 1)
         pick = jnp.where((row < local) & (column == row + first), 1.0, 0.0).astype(BF16)
         slab = w_dt_ref[:, pl.ds(slab_start, width)]
         w_rate = dot(pick, slab).astype(BF16)
-        lane = lax.broadcasted_iota(jnp.int32, (1, LANES), 1)
-        rate = dot_nt(scaled_ref[...], w_rate)
-        out_ref[:, start : start + LANES] = jnp.where(
-            lane == local, squares_ref[...], rate
-        ).astype(BF16)
+        ones = jnp.ones((RATE_ROWS, width), BF16)
+        squares = dot_nt(ones, squares_ref[0]) + dot_nt(ones, squares_ref[1])
+        out_row = lax.broadcasted_iota(jnp.int32, (RATE_ROWS, 1), 0)
+        rate = dot_nt(w_rate, scaled_ref[...])
+        rate_ref[...] = jnp.where(out_row == local, squares, rate).astype(BF16)
 
 
 def project(differences, tokens, tp_count, gain, weights, w_dt=None):
     props, _, seqs, width = tokens.shape
     rows = len(differences) * props * seqs
     columns = sum(weight.shape[1] for weight in weights)
+    outs = [jax.ShapeDtypeStruct((rows, columns), BF16)]
     scratch = [pltpu.VMEM((rows, width), BF16)]
     operands = [tokens, gain]
     if w_dt is not None:
-        columns += LANES
-        scratch.append(pltpu.VMEM((rows, 1), F32))
+        outs.append(jax.ShapeDtypeStruct((RATE_ROWS, rows), BF16))
+        scratch.append(pltpu.VMEM((2, rows, width), BF16))
         operands.append(w_dt)
     operands += list(weights)
     return pl.pallas_call(
         functools.partial(project_kernel, tuple(differences), w_dt is not None, tp_count),
-        out_shape=jax.ShapeDtypeStruct((rows, columns), BF16),
+        out_shape=outs,
         in_specs=whole(len(operands)),
-        out_specs=pl.BlockSpec(memory_space=VMEM),
+        out_specs=whole(len(outs)),
         scratch_shapes=scratch,
         cost_estimate=cost(2),
     )(*operands)
@@ -334,6 +338,7 @@
         a_log_ref,
         skip_ref,
         state_ref,
+        extra_ref,
         out_ref,
         scale_ref,
         post_x_ref,
@@ -346,8 +351,7 @@
     state_dim = state_ref.shape[3]
     groups = local_heads // HPG
     group_width = HPG * head_dim
-    rate_start = 2 * group_cols
-    extra = added(bcr_refs, slice(rate_start, rate_start + LANES))
+    extra = extra_ref[...]
     empty = jnp.zeros((1, LANES - local_heads), F32)
     bias = jnp.concatenate([bias_ref[...], empty], axis=1)
     a_rate = jnp.concatenate([-jnp.exp(a_log_ref[...]), empty], axis=1)
@@ -502,10 +506,13 @@
     return lax.optimization_barrier((value, *others))[0]
 
 
-def halving(addends, bit, blocks, *others):
-    half = addends[-1].shape[0] // 2
+def halving(addends, bit, blocks, *others, axis=0):
+    half = addends[-1].shape[axis] // 2
     addends = [*addends[:-1], after(addends[-1], *others)]
-    send = sum(addend[half : 2 * half].astype(F32) for addend in addends).astype(BF16)
+    send = sum(
+        lax.slice_in_dim(addend, half, 2 * half, axis=axis).astype(F32)
+        for addend in addends
+    ).astype(BF16)
     return send, [*addends, swap_bit(send, bit, blocks)]
 
 
@@ -567,14 +574,15 @@
     bcr_args = (tp_count, gains, [w_b, w_c], w_dt_t)
     x_args = (tp_count, gains, [w_x])
     z_args = (tp_count, gains, [w_z])
-    send_bcr = project(of_z[half:], tokens_q, *bcr_args)
+    send_bcr, send_rate = project(of_z[half:], tokens_q, *bcr_args)
     got_bcr = swap_bit(send_bcr, z_first[0], kv_count)
-    send_x = project(of_x[half:], after(tokens_q, send_bcr), *x_args)
+    (send_x,) = project(of_x[half:], after(tokens_q, send_bcr), *x_args)
     got_x = swap_bit(send_x, x_first[0], kv_count)
-    send_z = project(of_x[half:], after(tokens_q, send_x), *z_args)
+    (send_z,) = project(of_x[half:], after(tokens_q, send_x), *z_args)
     got_z = swap_bit(send_z, x_first[0], kv_count)
-    keep_bcr = project(of_z[:half], after(tokens_q, send_z), *bcr_args)
-    keep_x = project(of_x[:half], after(tokens_q, keep_bcr), *x_args)
+    got_rate = swap_bit(send_rate, z_first[0], kv_count)
+    keep_bcr, keep_rate = project(of_z[:half], after(tokens_q, send_z), *bcr_args)
+    (keep_x,) = project(of_x[:half], after(tokens_q, keep_bcr), *x_args)
 
     accepted = accepted[None, :]
     conv_x, conv_b, conv_c = by_position(conv_x), by_position(conv_b), by_position(conv_c)
@@ -586,9 +594,10 @@
     )
     sent_bcr, bcr = halving([keep_bcr, got_bcr], z_first[1], kv_count, links)
     sent_x, x = halving([keep_x, got_x], x_first[1], kv_count, sent_bcr)
-    keep_z = project(of_x[:half], after(tokens_q, sent_x), *z_args)
+    (keep_z,) = project(of_x[:half], after(tokens_q, sent_x), *z_args)
+    sent_rate, rate = halving([keep_rate, got_rate], z_first[1], kv_count, keep_z, axis=1)
     new_state, half_state = replay_state(
-        after(accepted, keep_z),
+        after(accepted, sent_rate),
         by_position(path_dt),
         dt_bias[None, :],
         a_log[None, :],
@@ -604,8 +613,12 @@
     for place in range(2, len(x_first)):
         sent_x, x = halving(x, x_first[place], kv_count, sent_z)
         sent_bcr, bcr = halving(bcr, z_first[place], kv_count, sent_x)
-        sent_z, z = halving(z, x_first[place], kv_count, sent_bcr)
-
+        sent_rate, rate = halving(rate, z_first[place], kv_count, sent_bcr, axis=1)
+        sent_z, z = halving(z, x_first[place], kv_count, sent_rate)
+
+    rate[-1] = after(rate[-1], sent_z)
+    extra = sum(addend[:, :rows_local].astype(F32) for addend in rate).T
+    extra = jnp.pad(extra, ((0, 0), (0, LANES - RATE_ROWS)))
     heads_out, row_scale = mix(
         seq_local,
         width,
@@ -623,6 +636,7 @@
             a_log[None, :],
             d_skip[None, :],
             half_state,
+            extra,
         ],
     )
     gated = gate(HPG * head_dim, z, row_scale, heads_out, gain_out[None, :])

time: 121 us -> 120 us (level)
  waiting for transfers between devices: 46.1 us -> 38.9 us
  starting transfers between devices: 20.2 us -> 26.1 us
    ppermute x13 -> x16, waiting for transfers between devices: 39.2 us -> 32 us  [swap_bit(): return lax.ppermute(array, 'kv', [(i, i ^ 1 << bit) for i in range(blocks)])]
    ppermute x13 -> x16, starting transfers between devices: 14.3 us -> 19.9 us  [swap_bit(): return lax.ppermute(array, 'kv', [(i, i ^ 1 << bit) for i in range(blocks)])]
    convert_element_type x6 -> x8, other arithmetic: 7.56 us -> 8.35 us  [halving(): send = sum((lax.slice_in_dim(addend, half, 2 * half, axis=axis).astype(F3...]
  transfers between devices with their start and end apart: 16 -> 19, of which waited for: 10 -> 9; matrix products, arithmetic and copies ran while one was open for 8% -> 10% of each run, Pallas kernels for 29% -> 29%
where the time goes in v2:
time: 120 us; the launch traced here: 118 us
  waiting for transfers between devices  38.9 us (32%)
  Pallas kernels  37.5 us (31%)
  starting transfers between devices  26.1 us (22%)
  other arithmetic  10.6 us (9%)
  local copies, waits for them, and re-layouts  2.35 us (2%)
  matrix products  1.89 us (2%)
    ppermute x16, waiting for transfers between devices, swap_bit(): return lax.ppermute(array, 'kv', [(i, i ^ 1 << bit) for i in range(blocks)])  32 us
    ppermute x16, starting transfers between devices, swap_bit(): return lax.ppermute(array, 'kv', [(i, i ^ 1 << bit) for i in range(blocks)])  19.9 us
    pallas_call x6, Pallas kernels, project(): pl.pallas_call(functools.partial(project_kernel, tuple(differences), w_dt...  18.1 us
    pallas_call x1, Pallas kernels, replay_state(): pl.pallas_call(state_kernel, grid=(seqs,), out_shape=[jax.ShapeDtypeStruc...  8.63 us
    convert_element_type x8, other arithmetic, halving(): send = sum((lax.slice_in_dim(addend, half, 2 * half, axis=axis).astype(F3...  8.35 us
    ppermute x2, starting transfers between devices, mixer(): total = total + lax.ppermute(piece, ('kv', 'tp'), route).astype(F32)  6.08 us
    ppermute x2, waiting for transfers between devices, mixer(): total = total + lax.ppermute(piece, ('kv', 'tp'), route).astype(F32)  5.27 us
    pallas_call x1, Pallas kernels, mix(): pl.pallas_call(functools.partial(mix_kernel, seqs, width, local_heads, le...  4.98 us
  transfers between devices with their start and end apart: 19, of which 9 were waited for; matrix products, arithmetic and copies ran while one was open for 10% of the time, Pallas kernels for 29%

profile of v2, /device:TPU:0, one launch (start us, length us, event | category | flops | bytes accessed | tf_op | source)
XLA Modules:
  0.0 118.2 jit_solution(2482585828825788517)
XLA Ops:
  0.6 3.1 %shard_map.248 = (bf16[384,1024]{1,0:T(8,128)(2,1)}, bf16[32,384]{1,0:T(8,128)(2,1)}) custom-call(bf16[12,8,8,512]{3,2,1,0:T(8,128)(2,1)} %bitcast.46, f32[1,4096]{1,0:T(1,128)} %bitcast.55, bf16[64,4096]{1,0:T(8,128)(2,1)} %bitcast.52, bf16[512,512]{1,0:T(8,128)(2,1)} %refs_1_.3, bf16[512,512]{1,0:T(8,128)(2,1)} %refs_2_.4), custom_call_target="tpu_custom_call" | custom-call | flops 8000000 | bytes 1024 | tf_op jit(solution)/shard_map/pallas_call | solution.py:113
  3.7 3.1 %collective-permute-start.1 = (bf16[384,1024]{1,0:T(8,128)(2,1)}, bf16[384,1024]{1,0:T(8,128)(2,1)S(1)}, u32[]{:S(2)}, u32[]{:S(2)}) collective-permute-start(bf16[384,1024]{1,0:T(8,128)(2,1)} %get-tuple-element.34), channel_id=1, source_target_pairs={{0,8},{4,12},{8,0},{12,4},{16,24},{20,28},{24,16},{28,20},{1,9},{5... | collective-permute-start | bytes 2359304 | tf_op jit(solution)/shard_map/ppermute | solution.py:502
  6.8 2.9 %shard_map.249 = bf16[384,1024]{1,0:T(8,128)(2,1)} custom-call(bf16[12,8,8,512]{3,2,1,0:T(8,128)(2,1)} %bitcast.47, f32[1,4096]{1,0:T(1,128)} %bitcast.56, bf16[512,1024]{1,0:T(8,128)(2,1)} %refs_0_.6), custom_call_target="tpu_custom_call" | custom-call | flops 8000000 | bytes 1024 | tf_op jit(solution)/shard_map/pallas_call | solution.py:113
  9.7 1.5 %collective-permute-start = (bf16[384,1024]{1,0:T(8,128)(2,1)}, bf16[384,1024]{1,0:T(8,128)(2,1)S(1)}, u32[]{:S(2)}, u32[]{:S(2)}) collective-permute-start(bf16[384,1024]{1,0:T(8,128)(2,1)} %shard_map.249), channel_id=1, source_target_pairs={{0,4},{4,0},{8,12},{12,8},{16,20},{20,16},{24,28},{28,24},{1,5},{5... | collective-permute-start | bytes 2359304 | tf_op jit(solution)/shard_map/ppermute | solution.py:502
  11.2 3.0 %shard_map.250 = bf16[384,1024]{1,0:T(8,128)(2,1)} custom-call(bf16[12,8,8,512]{3,2,1,0:T(8,128)(2,1)} %bitcast.48, f32[1,4096]{1,0:T(1,128)} %bitcast.57, bf16[512,1024]{1,0:T(8,128)(2,1)} %refs_0_.7), custom_call_target="tpu_custom_call" | custom-call | flops 8000000 | bytes 1024 | tf_op jit(solution)/shard_map/pallas_call | solution.py:113
  14.9 3.1 %shard_map.251 = (bf16[384,1024]{1,0:T(8,128)(2,1)}, bf16[32,384]{1,0:T(8,128)(2,1)}) custom-call(bf16[12,8,8,512]{3,2,1,0:T(8,128)(2,1)} %bitcast.49, f32[1,4096]{1,0:T(1,128)} %bitcast.58, bf16[64,4096]{1,0:T(8,128)(2,1)} %bitcast.53, bf16[512,512]{1,0:T(8,128)(2,1)} %refs_1_.3, bf16[512,512]{1,0:T(8,128)(2,1)} %refs_2_.4), custom_call_target="tpu_custom_call" | custom-call | flops 8000000 | bytes 1024 | tf_op jit(solution)/shard_map/pallas_call | solution.py:113
  18.0 3.0 %shard_map.252.refs_4_ = bf16[384,1024]{1,0:T(8,128)(2,1)} custom-call(bf16[12,8,8,512]{3,2,1,0:T(8,128)(2,1)} %bitcast.50, f32[1,4096]{1,0:T(1,128)} %bitcast.59, bf16[512,1024]{1,0:T(8,128)(2,1)} %refs_0_.6), custom_call_target="tpu_custom_call" | custom-call | flops 8000000 | bytes 1024 | tf_op jit(solution)/shard_map/pallas_call | solution.py:113
  21.2 3.5 %tree.1 = (bf16[288,96]{1,0:T(8,128)(2,1)}, f32[96,96]{1,0:T(8,128)}, f32[96,2048]{1,0:T(8,128)}) custom-call(s32[8,12]{1,0:T(8,128)} %parents_ref.1, s32[1,8]{1,0:T(1,128)} %bitcast.73, bf16[24,1024]{1,0:T(8,128)(2,1)} %bitcast.63, bf16[48,1024]{1,0:T(8,128)(2,1)} %bitcast.61, bf16[4,1024]{1,0:T(4,128)(2,1)} %refs_11_.1, bf16[24,512]{1,0:T(8,128)(2,1)} %bitcast.67, ...), custom_call_target="tpu_custom_call" | custom-call | flops 16000000 | bytes 1024 | tf_op jit(solution)/shard_map/tree/pallas_call | solution.py:303
  26.4 3.9 %collective-permute-done.refs_5_ = bf16[384,1024]{1,0:T(8,128)(2,1)S(1)} collective-permute-done((bf16[384,1024]{1,0:T(8,128)(2,1)}, bf16[384,1024]{1,0:T(8,128)(2,1)S(1)}, u32[]{:S(2)}, u32[]{:S(2)}) %collective-permute-start) | collective-permute-done | bytes 786464 | tf_op jit(solution)/shard_map/ppermute | solution.py:502
  30.4 2.1 %add_convert_fusion.2 = bf16[192,1024]{1,0:T(8,128)(2,1)} fusion(bf16[384,1024]{1,0:T(8,128)(2,1)} %shard_map.252.refs_4_, bf16[384,1024]{1,0:T(8,128)(2,1)S(1)} %collective-permute-done.refs_5_), kind=kLoop, calls=%fused_computation.9 | loop fusion | flops 786432 | bytes 1179648 | tf_op jit(solution)/shard_map/convert_element_type | solution.py:515
  32.5 3.0 %collective-permute-start.6 = (bf16[192,1024]{1,0:T(8,128)(2,1)}, bf16[192,1024]{1,0:T(8,128)(2,1)}, u32[]{:S(2)}, u32[]{:S(2)}) collective-permute-start(bf16[192,1024]{1,0:T(8,128)(2,1)} %add_convert_fusion.3), channel_id=1, source_target_pairs={{0,16},{4,20},{8,24},{12,28},{16,0},{20,4},{24,8},{28,12},{1,17},{... | collective-permute-start | bytes 1179656 | tf_op jit(solution)/shard_map/ppermute | solution.py:502
  35.5 2.9 %shard_map.253.refs_0_ = bf16[384,1024]{1,0:T(8,128)(2,1)} custom-call(bf16[12,8,8,512]{3,2,1,0:T(8,128)(2,1)} %bitcast.51, f32[1,4096]{1,0:T(1,128)} %bitcast.60, bf16[512,1024]{1,0:T(8,128)(2,1)} %refs_0_.7), custom_call_target="tpu_custom_call" | custom-call | flops 8000000 | bytes 1024 | tf_op jit(solution)/shard_map/pallas_call | solution.py:113
  39.1 8.6 %replay_state.1 = (f32[8,16,64,128]{3,2,1,0:T(8,128)}, bf16[8,16,64,128]{3,2,1,0:T(8,128)(2,1)}) custom-call(s32[1,8]{1,0:T(1,128)} %bitcast.74, bf16[48,16]{1,0:T(8,128)(2,1)} %bitcast.71, f32[1,16]{1,0:T(1,128)} %bitcast.75, f32[1,16]{1,0:T(1,128)} %bitcast.77, bf16[24,1024]{1,0:T(8,128)(2,1)} %bitcast.64, bf16[48,1024]{1,0:T(8,128)(2,1)} %bitcast.62, ...), custom_call_target="tpu_custom_call" | custom-call | flops 32000000 | bytes 1024 | tf_op jit(solution)/shard_map/replay_state/pallas_call | solution.py:228
  47.8 1.2 %add_convert_fusion.1 = bf16[192,1024]{1,0:T(8,128)(2,1)S(1)} fusion(bf16[384,1024]{1,0:T(8,128)(2,1)S(1)} %copy-done, bf16[384,1024]{1,0:T(8,128)(2,1)} %collective-permute-done.2.refs_1_), kind=kLoop, calls=%fused_computation.8 | loop fusion | flops 786432 | bytes 1179648 | tf_op jit(solution)/shard_map/convert_element_type | solution.py:515
  49.0 1.6 %collective-permute-start.4 = (bf16[192,1024]{1,0:T(8,128)(2,1)S(1)}, bf16[192,1024]{1,0:T(8,128)(2,1)S(1)}, u32[]{:S(2)}, u32[]{:S(2)}) collective-permute-start(bf16[192,1024]{1,0:T(8,128)(2,1)S(1)} %add_convert_fusion.1), channel_id=1, source_target_pairs={{0,8},{4,12},{8,0},{12,4},{16,24},{20,28},{24,16},{28,20},{1,9},{5... | collective-permute-start | bytes 1179656 | tf_op jit(solution)/shard_map/ppermute | solution.py:502
  50.6 1.1 add_convert_fusion.7
  52.8 1.6 %collective-permute-start.13 = (bf16[1024,512]{1,0:T(8,128)(2,1)}, bf16[1024,512]{1,0:T(8,128)(2,1)S(1)}, u32[]{:S(2)}, u32[]{:S(2)}) collective-permute-start(bf16[1024,512]{1,0:T(8,128)(2,1)} %param.49), channel_id=1, source_target_pairs={{0,4},{4,0},{8,12},{12,8},{16,20},{20,16},{24,28},{28,24},{1,5},{5... | collective-permute-start | bytes 3145736 | tf_op jit(solution)/shard_map/ppermute | solution.py:502
  54.7 2.6 %collective-permute-start.10 = (bf16[96,1024]{1,0:T(8,128)(2,1)S(1)}, bf16[96,1024]{1,0:T(8,128)(2,1)S(1)}, u32[]{:S(2)}, u32[]{:S(2)}) collective-permute-start(bf16[96,1024]{1,0:T(8,128)(2,1)S(1)} %add_convert_fusion.7), channel_id=1, source_target_pairs={{0,16},{4,20},{8,24},{12,28},{16,0},{20,4},{24,8},{28,12},{1,17},{... | collective-permute-start | bytes 589832 | tf_op jit(solution)/shard_map/ppermute | solution.py:502
  57.8 2.1 %collective-permute-done.5 = bf16[32,192]{0,1:T(8,128)(2,1)S(1)} collective-permute-done((bf16[32,192]{0,1:T(8,128)(2,1)S(1)}, bf16[32,192]{0,1:T(8,128)(2,1)S(1)}, u32[]{:S(2)}, u32[]{:S(2)}) %collective-permute-start.5) | collective-permute-done | bytes 12320 | tf_op jit(solution)/shard_map/ppermute | solution.py:502
  60.7 1.1 collective-permute-done.4.refs_2_
  61.7 1.1 add_convert_fusion.5
  62.9 2.5 %collective-permute-start.8 = (bf16[96,1024]{1,0:T(8,128)(2,1)S(1)}, bf16[96,1024]{1,0:T(8,128)(2,1)S(1)}, u32[]{:S(2)}, u32[]{:S(2)}) collective-permute-start(bf16[96,1024]{1,0:T(8,128)(2,1)S(1)} %add_convert_fusion.5), channel_id=1, source_target_pairs={{0,16},{4,20},{8,24},{12,28},{16,0},{20,4},{24,8},{28,12},{1,17},{... | collective-permute-start | bytes 589832 | tf_op jit(solution)/shard_map/ppermute | solution.py:502
  65.4 15.2 %collective-permute-done.11 = bf16[32,96]{0,1:T(8,128)(2,1)S(1)} collective-permute-done((bf16[32,96]{0,1:T(8,128)(2,1)S(1)}, bf16[32,96]{0,1:T(8,128)(2,1)S(1)}, u32[]{:S(2)}, u32[]{:S(2)}) %collective-permute-start.11) | collective-permute-done | bytes 6176 | tf_op jit(solution)/shard_map/ppermute | solution.py:502
  81.9 5.0 %mix.1 = (f32[96,1024]{1,0:T(8,128)}, f32[96,128]{1,0:T(8,128)}) custom-call(bf16[384,1024]{1,0:T(8,128)(2,1)} %get-tuple-element.38.refs_0_, bf16[384,1024]{1,0:T(8,128)(2,1)} %copy-done.1, bf16[192,1024]{1,0:T(8,128)(2,1)} %collective-permute-done.6.refs_2_, bf16[96,1024]{1,0:T(8,128)(2,1)} %copy-done.10, bf16[384,1024]{1,0:T(8,128)(2,1)} %shard_map.252.refs_4_, ...), custom_call_target="tpu_custom_call" | custom-call | flops 32000000 | bytes 1024 | tf_op jit(solution)/shard_map/mix/pallas_call | solution.py:461
  87.6 2.3 %gate.1 = bf16[96,1024]{1,0:T(8,128)(2,1)} custom-call(bf16[384,1024]{1,0:T(8,128)(2,1)} %shard_map.253.refs_0_, bf16[384,1024]{1,0:T(8,128)(2,1)} %collective-permute-done.2.refs_1_, bf16[192,1024]{1,0:T(8,128)(2,1)} %copy-done.5, bf16[96,1024]{1,0:T(8,128)(2,1)} %copy-done.11, f32[96,128]{1,0:T(8,128)} %get-tuple-element.60.refs_4_, ...), custom_call_target="tpu_custom_call" | custom-call | flops 4000000 | bytes 1024 | tf_op jit(solution)/shard_map/gate/pallas_call | solution.py:490
  90.2 1.6 %collective-permute-start.12 = (bf16[96,1024]{1,0:T(8,128)(2,1)}, bf16[96,1024]{1,0:T(8,128)(2,1)S(1)}, u32[]{:S(2)}, u32[]{:S(2)}) collective-permute-start(bf16[96,1024]{1,0:T(8,128)(2,1)} %gate.1), channel_id=1, source_target_pairs={{0,8},{4,12},{8,0},{12,4},{16,24},{20,28},{24,16},{28,20},{1,9},{5... | collective-permute-start | bytes 589832 | tf_op jit(solution)/shard_map/ppermute | solution.py:502
  91.8 6.2 %collective-permute-done.14 = bf16[96,1024]{1,0:T(8,128)(2,1)S(1)} collective-permute-done((bf16[96,1024]{1,0:T(8,128)(2,1)}, bf16[96,1024]{1,0:T(8,128)(2,1)S(1)}, u32[]{:S(2)}, u32[]{:S(2)}) %collective-permute-start.14) | collective-permute-done | bytes 196640 | tf_op jit(solution)/shard_map/ppermute | solution.py:502
  98.0 1.4 %broadcast_select_fusion.1 = (bf16[1024,512]{1,0:T(8,128)(2,1)S(1)}, bf16[1024,512]{1,0:T(8,128)(2,1)S(1)}) fusion(bf16[1024,512]{1,0:T(8,128)(2,1)S(1)} %collective-permute-done.13, bf16[1024,512]{1,0:T(8,128)(2,1)} %param.49, pred[]{:T(512)S(6)} %eq.7), kind=kLoop, calls=%fused_computation.6 | loop fusion | flops 1048576 | bytes 4194305 | tf_op jit(solution)/shard_map/jit(_where)/select_n | solution.py:652
  100.8 2.8 %collective-permute-done.15 = bf16[96,1024]{1,0:T(8,128)(2,1)S(1)} collective-permute-done((bf16[96,1024]{1,0:T(8,128)(2,1)S(1)}, bf16[96,1024]{1,0:T(8,128)(2,1)S(1)}, u32[]{:S(2)}, u32[]{:S(2)}) %collective-permute-start.15) | collective-permute-done | bytes 196640 | tf_op jit(solution)/shard_map/ppermute | solution.py:502
  104.3 1.7 %collective-permute-done.16 = bf16[192,1024]{1,0:T(8,128)(2,1)S(1)} collective-permute-done((bf16[192,1024]{1,0:T(8,128)(2,1)S(1)}, bf16[192,1024]{1,0:T(8,128)(2,1)S(1)}, u32[]{:S(2)}, u32[]{:S(2)}) %collective-permute-start.16) | collective-permute-done | bytes 393248 | tf_op jit(solution)/shard_map/ppermute | solution.py:668
  106.8 5.4 %collective-permute-start.18 = (bf16[96,1024]{1,0:T(8,128)(2,1)S(1)}, bf16[96,1024]{1,0:T(8,128)(2,1)S(1)}, u32[]{:S(2)}, u32[]{:S(2)}) collective-permute-start(bf16[96,1024]{1,0:T(8,128)(2,1)S(1)} %get-tuple-element.69), channel_id=1, source_target_pairs={{0,16},{1,24},{2,0},{3,8},{4,20},{5,28},{6,4},{7,12},{8,17},{9,25}... | collective-permute-start | bytes 589832 | tf_op jit(solution)/shard_map/ppermute | solution.py:687
  112.2 5.3 %collective-permute-done.18 = bf16[96,1024]{1,0:T(8,128)(2,1)S(1)} collective-permute-done((bf16[96,1024]{1,0:T(8,128)(2,1)S(1)}, bf16[96,1024]{1,0:T(8,128)(2,1)S(1)}, u32[]{:S(2)}, u32[]{:S(2)}) %collective-permute-start.18) | collective-permute-done | bytes 196640 | tf_op jit(solution)/shard_map/ppermute | solution.py:687
  (71 shorter events, 11.8 us)
Async XLA Ops:
  3.7 11.0 %copy-start.15 = (bf16[32,384]{1,0:T(8,128)(2,1)S(1)}, bf16[32,384]{1,0:T(8,128)(2,1)}, u32[]{:S(2)}) copy-start(bf16[32,384]{1,0:T(8,128)(2,1)} %get-tuple-element.46) | copy-start | bytes 73732
  3.7 21.7 %collective-permute-start.1 = (bf16[384,1024]{1,0:T(8,128)(2,1)}, bf16[384,1024]{1,0:T(8,128)(2,1)S(1)}, u32[]{:S(2)}, u32[]{:S(2)}) collective-permute-start(bf16[384,1024]{1,0:T(8,128)(2,1)} %get-tuple-element.34), channel_id=1, source_target_pairs={{0,8},{4,12},{8,0},{12,4},{16,24},{20,28},{24,16},{28,20},{1,9},{5... | collective-permute-start | bytes 2359304 | tf_op jit(solution)/shard_map/ppermute | solution.py:502
  9.7 20.6 %collective-permute-start = (bf16[384,1024]{1,0:T(8,128)(2,1)}, bf16[384,1024]{1,0:T(8,128)(2,1)S(1)}, u32[]{:S(2)}, u32[]{:S(2)}) collective-permute-start(bf16[384,1024]{1,0:T(8,128)(2,1)} %shard_map.249), channel_id=1, source_target_pairs={{0,4},{4,0},{8,12},{12,8},{16,20},{20,16},{24,28},{28,24},{1,5},{5... | collective-permute-start | bytes 2359304 | tf_op jit(solution)/shard_map/ppermute | solution.py:502
  14.2 33.6 %collective-permute-start.2 = (bf16[384,1024]{1,0:T(8,128)(2,1)}, bf16[384,1024]{1,0:T(8,128)(2,1)}, u32[]{:S(2)}, u32[]{:S(2)}) collective-permute-start(bf16[384,1024]{1,0:T(8,128)(2,1)} %shard_map.250), channel_id=1, source_target_pairs={{0,4},{4,0},{8,12},{12,8},{16,20},{20,16},{24,28},{28,24},{1,5},{5... | collective-permute-start | bytes 2359304 | tf_op jit(solution)/shard_map/ppermute | solution.py:502
  14.9 23.6 %collective-permute-start.3 = (bf16[32,384]{0,1:T(8,128)(2,1)S(1)}, bf16[32,384]{0,1:T(8,128)(2,1)S(1)}, u32[]{:S(2)}, u32[]{:S(2)}) collective-permute-start(bf16[32,384]{0,1:T(8,128)(2,1)S(1)} %copy.28), channel_id=1, source_target_pairs={{0,8},{4,12},{8,0},{12,4},{16,24},{20,28},{24,16},{28,20},{1,9},{5... | collective-permute-start | bytes 73736 | tf_op jit(solution)/shard_map/ppermute | solution.py:502
  18.0 3.0 %copy-start.16 = (bf16[32,384]{1,0:T(8,128)(2,1)S(1)}, bf16[32,384]{1,0:T(8,128)(2,1)}, u32[]{:S(2)}) copy-start(bf16[32,384]{1,0:T(8,128)(2,1)} %get-tuple-element.45) | copy-start | bytes 73732
  18.0 7.3 %copy-start.3 = (bf16[384,1024]{1,0:T(8,128)(2,1)S(1)}, bf16[384,1024]{1,0:T(8,128)(2,1)}, u32[]{:S(2)}) copy-start(bf16[384,1024]{1,0:T(8,128)(2,1)} %get-tuple-element.38.refs_0_) | copy-start | bytes 2359300
  21.2 17.3 %copy-start.6 = (bf16[32,384]{0,1:T(8,128)(2,1)}, bf16[32,384]{0,1:T(8,128)(2,1)S(1)}, u32[]{:S(2)}) copy-start(bf16[32,384]{0,1:T(8,128)(2,1)S(1)} %copy.27) | copy-start | bytes 73732
  25.4 26.4 %copy-start.1 = (bf16[384,1024]{1,0:T(8,128)(2,1)}, bf16[384,1024]{1,0:T(8,128)(2,1)S(1)}, u32[]{:S(2)}) copy-start(bf16[384,1024]{1,0:T(8,128)(2,1)S(1)} %collective-permute-done.1.refs_1_) | copy-start | bytes 2359300
  30.4 20.3 %copy-start.2 = (bf16[384,1024]{1,0:T(8,128)(2,1)}, bf16[384,1024]{1,0:T(8,128)(2,1)S(1)}, u32[]{:S(2)}) copy-start(bf16[384,1024]{1,0:T(8,128)(2,1)S(1)} %collective-permute-done.refs_5_) | copy-start | bytes 2359300
  32.5 18.1 %collective-permute-start.7 = (bf16[192,1024]{1,0:T(8,128)(2,1)}, bf16[192,1024]{1,0:T(8,128)(2,1)S(1)}, u32[]{:S(2)}, u32[]{:S(2)}) collective-permute-start(bf16[192,1024]{1,0:T(8,128)(2,1)} %add_convert_fusion.2), channel_id=1, source_target_pairs={{0,8},{4,12},{8,0},{12,4},{16,24},{20,28},{24,16},{28,20},{1,9},{5... | collective-permute-start | bytes 1179656 | tf_op jit(solution)/shard_map/ppermute | solution.py:502
  32.5 19.3 %collective-permute-start.6 = (bf16[192,1024]{1,0:T(8,128)(2,1)}, bf16[192,1024]{1,0:T(8,128)(2,1)}, u32[]{:S(2)}, u32[]{:S(2)}) collective-permute-start(bf16[192,1024]{1,0:T(8,128)(2,1)} %add_convert_fusion.3), channel_id=1, source_target_pairs={{0,16},{4,20},{8,24},{12,28},{16,0},{20,4},{24,8},{28,12},{1,17},{... | collective-permute-start | bytes 1179656 | tf_op jit(solution)/shard_map/ppermute | solution.py:502
  39.1 8.7 %copy-start = (bf16[384,1024]{1,0:T(8,128)(2,1)S(1)}, bf16[384,1024]{1,0:T(8,128)(2,1)}, u32[]{:S(2)}) copy-start(bf16[384,1024]{1,0:T(8,128)(2,1)} %shard_map.253.refs_0_) | copy-start | bytes 2359300
  47.8 6.6 %copy-start.14 = (bf16[32,192]{0,1:T(8,128)(2,1)S(1)}, bf16[32,192]{0,1:T(8,128)(2,1)}, u32[]{:S(2)}) copy-start(bf16[32,192]{0,1:T(8,128)(2,1)} %add_convert_fusion.8) | copy-start | bytes 36868
  47.8 12.1 %copy-start.7 = (bf16[32,384]{0,1:T(8,128)(2,1)S(1)}, bf16[32,384]{0,1:T(8,128)(2,1)}, u32[]{:S(2)}) copy-start(bf16[32,384]{0,1:T(8,128)(2,1)} %copy-done.6) | copy-start | bytes 73732
  47.8 12.1 %copy-start.13 = (bf16[32,384]{0,1:T(8,128)(2,1)S(1)}, bf16[32,384]{0,1:T(8,128)(2,1)}, u32[]{:S(2)}) copy-start(bf16[32,384]{0,1:T(8,128)(2,1)} %copy-done.12) | copy-start | bytes 73732
  49.0 12.7 %collective-permute-start.4 = (bf16[192,1024]{1,0:T(8,128)(2,1)S(1)}, bf16[192,1024]{1,0:T(8,128)(2,1)S(1)}, u32[]{:S(2)}, u32[]{:S(2)}) collective-permute-start(bf16[192,1024]{1,0:T(8,128)(2,1)S(1)} %add_convert_fusion.1), channel_id=1, source_target_pairs={{0,8},{4,12},{8,0},{12,4},{16,24},{20,28},{24,16},{28,20},{1,9},{5... | collective-permute-start | bytes 1179656 | tf_op jit(solution)/shard_map/ppermute | solution.py:502
  50.6 30.6 %copy-start.4 = (bf16[192,1024]{1,0:T(8,128)(2,1)}, bf16[192,1024]{1,0:T(8,128)(2,1)S(1)}, u32[]{:S(2)}) copy-start(bf16[192,1024]{1,0:T(8,128)(2,1)S(1)} %collective-permute-done.7.refs_6_) | copy-start | bytes 1179652
  52.8 45.2 %collective-permute-start.13 = (bf16[1024,512]{1,0:T(8,128)(2,1)}, bf16[1024,512]{1,0:T(8,128)(2,1)S(1)}, u32[]{:S(2)}, u32[]{:S(2)}) collective-permute-start(bf16[1024,512]{1,0:T(8,128)(2,1)} %param.49), channel_id=1, source_target_pairs={{0,4},{4,0},{8,12},{12,8},{16,20},{20,16},{24,28},{28,24},{1,5},{5... | collective-permute-start | bytes 3145736 | tf_op jit(solution)/shard_map/ppermute | solution.py:502
  54.4 5.5 %collective-permute-start.5 = (bf16[32,192]{0,1:T(8,128)(2,1)S(1)}, bf16[32,192]{0,1:T(8,128)(2,1)S(1)}, u32[]{:S(2)}, u32[]{:S(2)}) collective-permute-start(bf16[32,192]{0,1:T(8,128)(2,1)S(1)} %copy-done.14), channel_id=1, source_target_pairs={{0,16},{4,20},{8,24},{12,28},{16,0},{20,4},{24,8},{28,12},{1,17},{... | collective-permute-start | bytes 36872 | tf_op jit(solution)/shard_map/ppermute | solution.py:502
  54.7 26.4 %collective-permute-start.10 = (bf16[96,1024]{1,0:T(8,128)(2,1)S(1)}, bf16[96,1024]{1,0:T(8,128)(2,1)S(1)}, u32[]{:S(2)}, u32[]{:S(2)}) collective-permute-start(bf16[96,1024]{1,0:T(8,128)(2,1)S(1)} %add_convert_fusion.7), channel_id=1, source_target_pairs={{0,16},{4,20},{8,24},{12,28},{16,0},{20,4},{24,8},{28,12},{1,17},{... | collective-permute-start | bytes 589832 | tf_op jit(solution)/shard_map/ppermute | solution.py:502
  57.3 23.9 %collective-permute-start.9 = (bf16[96,1024]{1,0:T(8,128)(2,1)S(1)}, bf16[96,1024]{1,0:T(8,128)(2,1)S(1)}, u32[]{:S(2)}, u32[]{:S(2)}) collective-permute-start(bf16[96,1024]{1,0:T(8,128)(2,1)S(1)} %add_convert_fusion.6), channel_id=1, source_target_pairs={{0,4},{4,0},{8,12},{12,8},{16,20},{20,16},{24,28},{28,24},{1,5},{5... | collective-permute-start | bytes 589832 | tf_op jit(solution)/shard_map/ppermute | solution.py:502
  59.9 20.6 %collective-permute-start.11 = (bf16[32,96]{0,1:T(8,128)(2,1)S(1)}, bf16[32,96]{0,1:T(8,128)(2,1)S(1)}, u32[]{:S(2)}, u32[]{:S(2)}) collective-permute-start(bf16[32,96]{0,1:T(8,128)(2,1)S(1)} %add_convert_fusion.9), channel_id=1, source_target_pairs={{0,4},{4,0},{8,12},{12,8},{16,20},{20,16},{24,28},{28,24},{1,5},{5... | collective-permute-start | bytes 18440 | tf_op jit(solution)/shard_map/ppermute | solution.py:502
  61.7 1.2 copy-start.5
  62.9 24.0 %collective-permute-start.8 = (bf16[96,1024]{1,0:T(8,128)(2,1)S(1)}, bf16[96,1024]{1,0:T(8,128)(2,1)S(1)}, u32[]{:S(2)}, u32[]{:S(2)}) collective-permute-start(bf16[96,1024]{1,0:T(8,128)(2,1)S(1)} %add_convert_fusion.5), channel_id=1, source_target_pairs={{0,16},{4,20},{8,24},{12,28},{16,0},{20,4},{24,8},{28,12},{1,17},{... | collective-permute-start | bytes 589832 | tf_op jit(solution)/shard_map/ppermute | solution.py:502
  89.9 8.1 %collective-permute-start.14 = (bf16[96,1024]{1,0:T(8,128)(2,1)}, bf16[96,1024]{1,0:T(8,128)(2,1)S(1)}, u32[]{:S(2)}, u32[]{:S(2)}) collective-permute-start(bf16[96,1024]{1,0:T(8,128)(2,1)} %gate.1), channel_id=1, source_target_pairs={{0,16},{4,20},{8,24},{12,28},{16,0},{20,4},{24,8},{28,12},{1,17},{... | collective-permute-start | bytes 589832 | tf_op jit(solution)/shard_map/ppermute | solution.py:502
  90.2 9.2 %copy-start.8 = (bf16[96,1024]{1,0:T(8,128)(2,1)S(1)}, bf16[96,1024]{1,0:T(8,128)(2,1)}, u32[]{:S(2)}) copy-start(bf16[96,1024]{1,0:T(8,128)(2,1)} %gate.1) | copy-start | bytes 589828
  90.2 9.7 %collective-permute-start.12 = (bf16[96,1024]{1,0:T(8,128)(2,1)}, bf16[96,1024]{1,0:T(8,128)(2,1)S(1)}, u32[]{:S(2)}, u32[]{:S(2)}) collective-permute-start(bf16[96,1024]{1,0:T(8,128)(2,1)} %gate.1), channel_id=1, source_target_pairs={{0,8},{4,12},{8,0},{12,4},{16,24},{20,28},{24,16},{28,20},{1,9},{5... | collective-permute-start | bytes 589832 | tf_op jit(solution)/shard_map/ppermute | solution.py:502
  98.0 5.7 %collective-permute-start.15 = (bf16[96,1024]{1,0:T(8,128)(2,1)S(1)}, bf16[96,1024]{1,0:T(8,128)(2,1)S(1)}, u32[]{:S(2)}, u32[]{:S(2)}) collective-permute-start(bf16[96,1024]{1,0:T(8,128)(2,1)S(1)} %collective-permute-done.14), channel_id=1, source_target_pairs={{0,8},{4,12},{8,0},{12,4},{16,24},{20,28},{24,16},{28,20},{1,9},{5... | collective-permute-start | bytes 589832 | tf_op jit(solution)/shard_map/ppermute | solution.py:502
  104.2 1.8 %collective-permute-start.16 = (bf16[192,1024]{1,0:T(8,128)(2,1)S(1)}, bf16[192,1024]{1,0:T(8,128)(2,1)S(1)}, u32[]{:S(2)}, u32[]{:S(2)}) collective-permute-start(bf16[192,1024]{1,0:T(8,128)(2,1)S(1)} %pad_maximum_fusion.1), channel_id=1, source_target_pairs={{0,1},{1,0},{2,3},{3,2},{4,5},{5,4},{6,7},{7,6},{8,9},{9,8},{10,11... | collective-permute-start | bytes 1179656 | tf_op jit(solution)/shard_map/ppermute | solution.py:668
  106.1 6.1 %collective-permute-start.17 = (bf16[96,1024]{1,0:T(8,128)(2,1)S(1)}, bf16[96,1024]{1,0:T(8,128)(2,1)S(1)}, u32[]{:S(2)}, u32[]{:S(2)}) collective-permute-start(bf16[96,1024]{1,0:T(8,128)(2,1)S(1)} %get-tuple-element.68), channel_id=1, source_target_pairs={{0,0},{1,8},{2,16},{3,24},{4,4},{5,12},{6,20},{7,28},{8,1},{9,9},{... | collective-permute-start | bytes 589832 | tf_op jit(solution)/shard_map/ppermute | solution.py:687
  106.8 10.7 %collective-permute-start.18 = (bf16[96,1024]{1,0:T(8,128)(2,1)S(1)}, bf16[96,1024]{1,0:T(8,128)(2,1)S(1)}, u32[]{:S(2)}, u32[]{:S(2)}) collective-permute-start(bf16[96,1024]{1,0:T(8,128)(2,1)S(1)} %get-tuple-element.69), channel_id=1, source_target_pairs={{0,16},{1,24},{2,0},{3,8},{4,20},{5,28},{6,4},{7,12},{8,17},{9,25}... | collective-permute-start | bytes 589832 | tf_op jit(solution)/shard_map/ppermute | solution.py:687
  (4 other events, 2.8 us)

commit v3 on v2

--- a/solution.py
+++ b/solution.py
@@ -61,10 +61,15 @@
     me = lax.axis_index("kv")
     rows_local = props * seqs
     if with_rate:
-        w_dt_ref, *w_refs, out_ref, rate_ref, scaled_ref, squares_ref = refs
+        w_dt_ref, *w_refs, out_ref, rate_ref, scaled_ref, squares_ref, slab_ref, slab_sem = refs
     else:
         *w_refs, out_ref, scaled_ref = refs
     slab_start = pl.multiple_of(me * width, LANES)
+    if with_rate:
+        slab_copy = pltpu.make_async_copy(
+            w_dt_ref.at[:, pl.ds(slab_start, width)], slab_ref, slab_sem
+        )
+        slab_copy.start()
     gain = gain_ref[:, pl.ds(slab_start, width)]
     for position, difference in enumerate(differences):
         rows = tokens_ref[:, me ^ difference].astype(F32).reshape(rows_local, width)
@@ -89,8 +94,8 @@
         row = lax.broadcasted_iota(jnp.int32, (RATE_ROWS, heads), 0)
         column = lax.broadcasted_iota(jnp.int32, (RATE_ROWS, heads), 1)
         pick = jnp.where((row < local) & (column == row + first), 1.0, 0.0).astype(BF16)
-        slab = w_dt_ref[:, pl.ds(slab_start, width)]
-        w_rate = dot(pick, slab).astype(BF16)
+        slab_copy.wait()
+        w_rate = dot(pick, slab_ref[...]).astype(BF16)
         ones = jnp.ones((RATE_ROWS, width), BF16)
         squares = dot_nt(ones, squares_ref[0]) + dot_nt(ones, squares_ref[1])
         out_row = lax.broadcasted_iota(jnp.int32, (RATE_ROWS, 1), 0)
@@ -108,12 +113,17 @@
     if w_dt is not None:
         outs.append(jax.ShapeDtypeStruct((RATE_ROWS, rows), BF16))
         scratch.append(pltpu.VMEM((2, rows, width), BF16))
+        scratch.append(pltpu.VMEM((w_dt.shape[0], width), BF16))
+        scratch.append(pltpu.SemaphoreType.DMA)
         operands.append(w_dt)
     operands += list(weights)
+    specs = whole(len(operands))
+    if w_dt is not None:
+        specs[2] = pl.BlockSpec(memory_space=pl.ANY)
     return pl.pallas_call(
         functools.partial(project_kernel, tuple(differences), w_dt is not None, tp_count),
         out_shape=outs,
-        in_specs=whole(len(operands)),
+        in_specs=specs,
         out_specs=whole(len(outs)),
         scratch_shapes=scratch,
         cost_estimate=cost(2),

time: 120 us -> 121 us (level)
  no operation moved by 1% of the time
where the time goes in v3:
time: 121 us; the launch traced here: 119 us
  waiting for transfers between devices  38.6 us (32%)
  Pallas kernels  38.1 us (31%)
  starting transfers between devices  26.1 us (22%)
  other arithmetic  10.6 us (9%)
  local copies, waits for them, and re-layouts  2.35 us (2%)
  matrix products  1.89 us (2%)
    ppermute x16, waiting for transfers between devices, swap_bit(): return lax.ppermute(array, 'kv', [(i, i ^ 1 << bit) for i in range(blocks)])  31.6 us
    ppermute x16, starting transfers between devices, swap_bit(): return lax.ppermute(array, 'kv', [(i, i ^ 1 << bit) for i in range(blocks)])  20 us
    pallas_call x6, Pallas kernels, project(): pl.pallas_call(functools.partial(project_kernel, tuple(differences), w_dt...  18.7 us
    pallas_call x1, Pallas kernels, replay_state(): pl.pallas_call(state_kernel, grid=(seqs,), out_shape=[jax.ShapeDtypeStruc...  8.63 us
    convert_element_type x8, other arithmetic, halving(): send = sum((lax.slice_in_dim(addend, half, 2 * half, axis=axis).astype(F3...  8.35 us
    ppermute x2, starting transfers between devices, mixer(): total = total + lax.ppermute(piece, ('kv', 'tp'), route).astype(F32)  6.06 us
    ppermute x2, waiting for transfers between devices, mixer(): total = total + lax.ppermute(piece, ('kv', 'tp'), route).astype(F32)  5.28 us
    pallas_call x1, Pallas kernels, mix(): pl.pallas_call(functools.partial(mix_kernel, seqs, width, local_heads, le...  4.98 us
  transfers between devices with their start and end apart: 19, of which 9 were waited for; matrix products, arithmetic and copies ran while one was open for 10% of the time, Pallas kernels for 29%

profile of v3, /device:TPU:0, one launch (start us, length us, event | category | flops | bytes accessed | tf_op | source)
XLA Modules:
  0.0 118.6 jit_solution(11760336768533582587)
XLA Ops:
  0.6 3.4 %shard_map.248 = (bf16[384,1024]{1,0:T(8,128)(2,1)}, bf16[32,384]{1,0:T(8,128)(2,1)}) custom-call(bf16[12,8,8,512]{3,2,1,0:T(8,128)(2,1)} %bitcast.46, f32[1,4096]{1,0:T(1,128)} %bitcast.55, bf16[64,4096]{1,0:T(8,128)(2,1)} %bitcast.52, bf16[512,512]{1,0:T(8,128)(2,1)} %refs_1_.3, bf16[512,512]{1,0:T(8,128)(2,1)} %refs_2_.4), custom_call_target="tpu_custom_call" | custom-call | flops 8000000 | bytes 1024 | tf_op jit(solution)/shard_map/pallas_call | solution.py:123
  4.0 3.1 %collective-permute-start.1 = (bf16[384,1024]{1,0:T(8,128)(2,1)}, bf16[384,1024]{1,0:T(8,128)(2,1)S(1)}, u32[]{:S(2)}, u32[]{:S(2)}) collective-permute-start(bf16[384,1024]{1,0:T(8,128)(2,1)} %get-tuple-element.34), channel_id=1, source_target_pairs={{0,8},{4,12},{8,0},{12,4},{16,24},{20,28},{24,16},{28,20},{1,9},{5... | collective-permute-start | bytes 2359304 | tf_op jit(solution)/shard_map/ppermute | solution.py:512
  7.2 2.9 %shard_map.249 = bf16[384,1024]{1,0:T(8,128)(2,1)} custom-call(bf16[12,8,8,512]{3,2,1,0:T(8,128)(2,1)} %bitcast.47, f32[1,4096]{1,0:T(1,128)} %bitcast.56, bf16[512,1024]{1,0:T(8,128)(2,1)} %refs_0_.6), custom_call_target="tpu_custom_call" | custom-call | flops 8000000 | bytes 1024 | tf_op jit(solution)/shard_map/pallas_call | solution.py:123
  10.1 1.5 %collective-permute-start = (bf16[384,1024]{1,0:T(8,128)(2,1)}, bf16[384,1024]{1,0:T(8,128)(2,1)S(1)}, u32[]{:S(2)}, u32[]{:S(2)}) collective-permute-start(bf16[384,1024]{1,0:T(8,128)(2,1)} %shard_map.249), channel_id=1, source_target_pairs={{0,4},{4,0},{8,12},{12,8},{16,20},{20,16},{24,28},{28,24},{1,5},{5... | collective-permute-start | bytes 2359304 | tf_op jit(solution)/shard_map/ppermute | solution.py:512
  11.6 3.0 %shard_map.250 = bf16[384,1024]{1,0:T(8,128)(2,1)} custom-call(bf16[12,8,8,512]{3,2,1,0:T(8,128)(2,1)} %bitcast.48, f32[1,4096]{1,0:T(1,128)} %bitcast.57, bf16[512,1024]{1,0:T(8,128)(2,1)} %refs_0_.7), custom_call_target="tpu_custom_call" | custom-call | flops 8000000 | bytes 1024 | tf_op jit(solution)/shard_map/pallas_call | solution.py:123
  15.3 3.4 %shard_map.251 = (bf16[384,1024]{1,0:T(8,128)(2,1)}, bf16[32,384]{1,0:T(8,128)(2,1)}) custom-call(bf16[12,8,8,512]{3,2,1,0:T(8,128)(2,1)} %bitcast.49, f32[1,4096]{1,0:T(1,128)} %bitcast.58, bf16[64,4096]{1,0:T(8,128)(2,1)} %bitcast.53, bf16[512,512]{1,0:T(8,128)(2,1)} %refs_1_.3, bf16[512,512]{1,0:T(8,128)(2,1)} %refs_2_.4), custom_call_target="tpu_custom_call" | custom-call | flops 8000000 | bytes 1024 | tf_op jit(solution)/shard_map/pallas_call | solution.py:123
  18.7 3.0 %shard_map.252.refs_4_ = bf16[384,1024]{1,0:T(8,128)(2,1)} custom-call(bf16[12,8,8,512]{3,2,1,0:T(8,128)(2,1)} %bitcast.50, f32[1,4096]{1,0:T(1,128)} %bitcast.59, bf16[512,1024]{1,0:T(8,128)(2,1)} %refs_0_.6), custom_call_target="tpu_custom_call" | custom-call | flops 8000000 | bytes 1024 | tf_op jit(solution)/shard_map/pallas_call | solution.py:123
  21.9 3.5 %tree.1 = (bf16[288,96]{1,0:T(8,128)(2,1)}, f32[96,96]{1,0:T(8,128)}, f32[96,2048]{1,0:T(8,128)}) custom-call(s32[8,12]{1,0:T(8,128)} %parents_ref.1, s32[1,8]{1,0:T(1,128)} %bitcast.73, bf16[24,1024]{1,0:T(8,128)(2,1)} %bitcast.63, bf16[48,1024]{1,0:T(8,128)(2,1)} %bitcast.61, bf16[4,1024]{1,0:T(4,128)(2,1)} %refs_11_.1, bf16[24,512]{1,0:T(8,128)(2,1)} %bitcast.67, ...), custom_call_target="tpu_custom_call" | custom-call | flops 16000000 | bytes 1024 | tf_op jit(solution)/shard_map/tree/pallas_call | solution.py:313
  26.8 3.9 %collective-permute-done.refs_5_ = bf16[384,1024]{1,0:T(8,128)(2,1)S(1)} collective-permute-done((bf16[384,1024]{1,0:T(8,128)(2,1)}, bf16[384,1024]{1,0:T(8,128)(2,1)S(1)}, u32[]{:S(2)}, u32[]{:S(2)}) %collective-permute-start) | collective-permute-done | bytes 786464 | tf_op jit(solution)/shard_map/ppermute | solution.py:512
  30.7 2.1 %add_convert_fusion.2 = bf16[192,1024]{1,0:T(8,128)(2,1)} fusion(bf16[384,1024]{1,0:T(8,128)(2,1)} %shard_map.252.refs_4_, bf16[384,1024]{1,0:T(8,128)(2,1)S(1)} %collective-permute-done.refs_5_), kind=kLoop, calls=%fused_computation.9 | loop fusion | flops 786432 | bytes 1179648 | tf_op jit(solution)/shard_map/convert_element_type | solution.py:525
  32.9 3.0 %collective-permute-start.6 = (bf16[192,1024]{1,0:T(8,128)(2,1)}, bf16[192,1024]{1,0:T(8,128)(2,1)}, u32[]{:S(2)}, u32[]{:S(2)}) collective-permute-start(bf16[192,1024]{1,0:T(8,128)(2,1)} %add_convert_fusion.3), channel_id=1, source_target_pairs={{0,16},{4,20},{8,24},{12,28},{16,0},{20,4},{24,8},{28,12},{1,17},{... | collective-permute-start | bytes 1179656 | tf_op jit(solution)/shard_map/ppermute | solution.py:512
  35.9 2.9 %shard_map.253.refs_0_ = bf16[384,1024]{1,0:T(8,128)(2,1)} custom-call(bf16[12,8,8,512]{3,2,1,0:T(8,128)(2,1)} %bitcast.51, f32[1,4096]{1,0:T(1,128)} %bitcast.60, bf16[512,1024]{1,0:T(8,128)(2,1)} %refs_0_.7), custom_call_target="tpu_custom_call" | custom-call | flops 8000000 | bytes 1024 | tf_op jit(solution)/shard_map/pallas_call | solution.py:123
  39.5 8.6 %replay_state.1 = (f32[8,16,64,128]{3,2,1,0:T(8,128)}, bf16[8,16,64,128]{3,2,1,0:T(8,128)(2,1)}) custom-call(s32[1,8]{1,0:T(1,128)} %bitcast.74, bf16[48,16]{1,0:T(8,128)(2,1)} %bitcast.71, f32[1,16]{1,0:T(1,128)} %bitcast.75, f32[1,16]{1,0:T(1,128)} %bitcast.77, bf16[24,1024]{1,0:T(8,128)(2,1)} %bitcast.64, bf16[48,1024]{1,0:T(8,128)(2,1)} %bitcast.62, ...), custom_call_target="tpu_custom_call" | custom-call | flops 32000000 | bytes 1024 | tf_op jit(solution)/shard_map/replay_state/pallas_call | solution.py:238
  48.2 1.2 %add_convert_fusion.1 = bf16[192,1024]{1,0:T(8,128)(2,1)S(1)} fusion(bf16[384,1024]{1,0:T(8,128)(2,1)S(1)} %copy-done, bf16[384,1024]{1,0:T(8,128)(2,1)} %collective-permute-done.2.refs_1_), kind=kLoop, calls=%fused_computation.8 | loop fusion | flops 786432 | bytes 1179648 | tf_op jit(solution)/shard_map/convert_element_type | solution.py:525
  49.4 1.6 %collective-permute-start.4 = (bf16[192,1024]{1,0:T(8,128)(2,1)S(1)}, bf16[192,1024]{1,0:T(8,128)(2,1)S(1)}, u32[]{:S(2)}, u32[]{:S(2)}) collective-permute-start(bf16[192,1024]{1,0:T(8,128)(2,1)S(1)} %add_convert_fusion.1), channel_id=1, source_target_pairs={{0,8},{4,12},{8,0},{12,4},{16,24},{20,28},{24,16},{28,20},{1,9},{5... | collective-permute-start | bytes 1179656 | tf_op jit(solution)/shard_map/ppermute | solution.py:512
  51.0 1.1 add_convert_fusion.7
  53.2 1.6 %collective-permute-start.13 = (bf16[1024,512]{1,0:T(8,128)(2,1)}, bf16[1024,512]{1,0:T(8,128)(2,1)S(1)}, u32[]{:S(2)}, u32[]{:S(2)}) collective-permute-start(bf16[1024,512]{1,0:T(8,128)(2,1)} %param.49), channel_id=1, source_target_pairs={{0,4},{4,0},{8,12},{12,8},{16,20},{20,16},{24,28},{28,24},{1,5},{5... | collective-permute-start | bytes 3145736 | tf_op jit(solution)/shard_map/ppermute | solution.py:512
  55.1 2.6 %collective-permute-start.10 = (bf16[96,1024]{1,0:T(8,128)(2,1)S(1)}, bf16[96,1024]{1,0:T(8,128)(2,1)S(1)}, u32[]{:S(2)}, u32[]{:S(2)}) collective-permute-start(bf16[96,1024]{1,0:T(8,128)(2,1)S(1)} %add_convert_fusion.7), channel_id=1, source_target_pairs={{0,16},{4,20},{8,24},{12,28},{16,0},{20,4},{24,8},{28,12},{1,17},{... | collective-permute-start | bytes 589832 | tf_op jit(solution)/shard_map/ppermute | solution.py:512
  58.2 2.1 %collective-permute-done.5 = bf16[32,192]{0,1:T(8,128)(2,1)S(1)} collective-permute-done((bf16[32,192]{0,1:T(8,128)(2,1)S(1)}, bf16[32,192]{0,1:T(8,128)(2,1)S(1)}, u32[]{:S(2)}, u32[]{:S(2)}) %collective-permute-start.5) | collective-permute-done | bytes 12320 | tf_op jit(solution)/shard_map/ppermute | solution.py:512
  61.0 1.1 collective-permute-done.4.refs_2_
  62.1 1.1 add_convert_fusion.5
  63.3 2.5 %collective-permute-start.8 = (bf16[96,1024]{1,0:T(8,128)(2,1)S(1)}, bf16[96,1024]{1,0:T(8,128)(2,1)S(1)}, u32[]{:S(2)}, u32[]{:S(2)}) collective-permute-start(bf16[96,1024]{1,0:T(8,128)(2,1)S(1)} %add_convert_fusion.5), channel_id=1, source_target_pairs={{0,16},{4,20},{8,24},{12,28},{16,0},{20,4},{24,8},{28,12},{1,17},{... | collective-permute-start | bytes 589832 | tf_op jit(solution)/shard_map/ppermute | solution.py:512
  65.7 15.2 %collective-permute-done.11 = bf16[32,96]{0,1:T(8,128)(2,1)S(1)} collective-permute-done((bf16[32,96]{0,1:T(8,128)(2,1)S(1)}, bf16[32,96]{0,1:T(8,128)(2,1)S(1)}, u32[]{:S(2)}, u32[]{:S(2)}) %collective-permute-start.11) | collective-permute-done | bytes 6176 | tf_op jit(solution)/shard_map/ppermute | solution.py:512
  82.3 5.0 %mix.1 = (f32[96,1024]{1,0:T(8,128)}, f32[96,128]{1,0:T(8,128)}) custom-call(bf16[384,1024]{1,0:T(8,128)(2,1)} %get-tuple-element.38.refs_0_, bf16[384,1024]{1,0:T(8,128)(2,1)} %copy-done.1, bf16[192,1024]{1,0:T(8,128)(2,1)} %collective-permute-done.6.refs_2_, bf16[96,1024]{1,0:T(8,128)(2,1)} %copy-done.10, bf16[384,1024]{1,0:T(8,128)(2,1)} %shard_map.252.refs_4_, ...), custom_call_target="tpu_custom_call" | custom-call | flops 32000000 | bytes 1024 | tf_op jit(solution)/shard_map/mix/pallas_call | solution.py:471
  87.9 2.3 %gate.1 = bf16[96,1024]{1,0:T(8,128)(2,1)} custom-call(bf16[384,1024]{1,0:T(8,128)(2,1)} %shard_map.253.refs_0_, bf16[384,1024]{1,0:T(8,128)(2,1)} %collective-permute-done.2.refs_1_, bf16[192,1024]{1,0:T(8,128)(2,1)} %copy-done.5, bf16[96,1024]{1,0:T(8,128)(2,1)} %copy-done.11, f32[96,128]{1,0:T(8,128)} %get-tuple-element.60.refs_4_, ...), custom_call_target="tpu_custom_call" | custom-call | flops 4000000 | bytes 1024 | tf_op jit(solution)/shard_map/gate/pallas_call | solution.py:500
  90.6 1.6 %collective-permute-start.12 = (bf16[96,1024]{1,0:T(8,128)(2,1)}, bf16[96,1024]{1,0:T(8,128)(2,1)S(1)}, u32[]{:S(2)}, u32[]{:S(2)}) collective-permute-start(bf16[96,1024]{1,0:T(8,128)(2,1)} %gate.1), channel_id=1, source_target_pairs={{0,8},{4,12},{8,0},{12,4},{16,24},{20,28},{24,16},{28,20},{1,9},{5... | collective-permute-start | bytes 589832 | tf_op jit(solution)/shard_map/ppermute | solution.py:512
  92.2 6.2 %collective-permute-done.14 = bf16[96,1024]{1,0:T(8,128)(2,1)S(1)} collective-permute-done((bf16[96,1024]{1,0:T(8,128)(2,1)}, bf16[96,1024]{1,0:T(8,128)(2,1)S(1)}, u32[]{:S(2)}, u32[]{:S(2)}) %collective-permute-start.14) | collective-permute-done | bytes 196640 | tf_op jit(solution)/shard_map/ppermute | solution.py:512
  98.4 1.4 %broadcast_select_fusion.1 = (bf16[1024,512]{1,0:T(8,128)(2,1)S(1)}, bf16[1024,512]{1,0:T(8,128)(2,1)S(1)}) fusion(bf16[1024,512]{1,0:T(8,128)(2,1)S(1)} %collective-permute-done.13, bf16[1024,512]{1,0:T(8,128)(2,1)} %param.49, pred[]{:T(512)S(6)} %eq.7), kind=kLoop, calls=%fused_computation.6 | loop fusion | flops 1048576 | bytes 4194305 | tf_op jit(solution)/shard_map/jit(_where)/select_n | solution.py:662
  101.2 2.8 %collective-permute-done.15 = bf16[96,1024]{1,0:T(8,128)(2,1)S(1)} collective-permute-done((bf16[96,1024]{1,0:T(8,128)(2,1)S(1)}, bf16[96,1024]{1,0:T(8,128)(2,1)S(1)}, u32[]{:S(2)}, u32[]{:S(2)}) %collective-permute-start.15) | collective-permute-done | bytes 196640 | tf_op jit(solution)/shard_map/ppermute | solution.py:512
  104.6 1.7 %collective-permute-done.16 = bf16[192,1024]{1,0:T(8,128)(2,1)S(1)} collective-permute-done((bf16[192,1024]{1,0:T(8,128)(2,1)S(1)}, bf16[192,1024]{1,0:T(8,128)(2,1)S(1)}, u32[]{:S(2)}, u32[]{:S(2)}) %collective-permute-start.16) | collective-permute-done | bytes 393248 | tf_op jit(solution)/shard_map/ppermute | solution.py:678
  107.2 5.4 %collective-permute-start.18 = (bf16[96,1024]{1,0:T(8,128)(2,1)S(1)}, bf16[96,1024]{1,0:T(8,128)(2,1)S(1)}, u32[]{:S(2)}, u32[]{:S(2)}) collective-permute-start(bf16[96,1024]{1,0:T(8,128)(2,1)S(1)} %get-tuple-element.69), channel_id=1, source_target_pairs={{0,16},{1,24},{2,0},{3,8},{4,20},{5,28},{6,4},{7,12},{8,17},{9,25}... | collective-permute-start | bytes 589832 | tf_op jit(solution)/shard_map/ppermute | solution.py:697
  112.6 5.3 %collective-permute-done.18 = bf16[96,1024]{1,0:T(8,128)(2,1)S(1)} collective-permute-done((bf16[96,1024]{1,0:T(8,128)(2,1)S(1)}, bf16[96,1024]{1,0:T(8,128)(2,1)S(1)}, u32[]{:S(2)}, u32[]{:S(2)}) %collective-permute-start.18) | collective-permute-done | bytes 196640 | tf_op jit(solution)/shard_map/ppermute | solution.py:697
  (71 shorter events, 11.5 us)
Async XLA Ops:
  4.0 11.1 %copy-start.15 = (bf16[32,384]{1,0:T(8,128)(2,1)S(1)}, bf16[32,384]{1,0:T(8,128)(2,1)}, u32[]{:S(2)}) copy-start(bf16[32,384]{1,0:T(8,128)(2,1)} %get-tuple-element.46) | copy-start | bytes 73732
  4.0 21.7 %collective-permute-start.1 = (bf16[384,1024]{1,0:T(8,128)(2,1)}, bf16[384,1024]{1,0:T(8,128)(2,1)S(1)}, u32[]{:S(2)}, u32[]{:S(2)}) collective-permute-start(bf16[384,1024]{1,0:T(8,128)(2,1)} %get-tuple-element.34), channel_id=1, source_target_pairs={{0,8},{4,12},{8,0},{12,4},{16,24},{20,28},{24,16},{28,20},{1,9},{5... | collective-permute-start | bytes 2359304 | tf_op jit(solution)/shard_map/ppermute | solution.py:512
  10.1 20.6 %collective-permute-start = (bf16[384,1024]{1,0:T(8,128)(2,1)}, bf16[384,1024]{1,0:T(8,128)(2,1)S(1)}, u32[]{:S(2)}, u32[]{:S(2)}) collective-permute-start(bf16[384,1024]{1,0:T(8,128)(2,1)} %shard_map.249), channel_id=1, source_target_pairs={{0,4},{4,0},{8,12},{12,8},{16,20},{20,16},{24,28},{28,24},{1,5},{5... | collective-permute-start | bytes 2359304 | tf_op jit(solution)/shard_map/ppermute | solution.py:512
  14.6 33.6 %collective-permute-start.2 = (bf16[384,1024]{1,0:T(8,128)(2,1)}, bf16[384,1024]{1,0:T(8,128)(2,1)}, u32[]{:S(2)}, u32[]{:S(2)}) collective-permute-start(bf16[384,1024]{1,0:T(8,128)(2,1)} %shard_map.250), channel_id=1, source_target_pairs={{0,4},{4,0},{8,12},{12,8},{16,20},{20,16},{24,28},{28,24},{1,5},{5... | collective-permute-start | bytes 2359304 | tf_op jit(solution)/shard_map/ppermute | solution.py:512
  15.2 23.6 %collective-permute-start.3 = (bf16[32,384]{0,1:T(8,128)(2,1)S(1)}, bf16[32,384]{0,1:T(8,128)(2,1)S(1)}, u32[]{:S(2)}, u32[]{:S(2)}) collective-permute-start(bf16[32,384]{0,1:T(8,128)(2,1)S(1)} %copy.28), channel_id=1, source_target_pairs={{0,8},{4,12},{8,0},{12,4},{16,24},{20,28},{24,16},{28,20},{1,9},{5... | collective-permute-start | bytes 73736 | tf_op jit(solution)/shard_map/ppermute | solution.py:512
  18.7 3.0 %copy-start.16 = (bf16[32,384]{1,0:T(8,128)(2,1)S(1)}, bf16[32,384]{1,0:T(8,128)(2,1)}, u32[]{:S(2)}) copy-start(bf16[32,384]{1,0:T(8,128)(2,1)} %get-tuple-element.45) | copy-start | bytes 73732
  18.7 7.0 %copy-start.3 = (bf16[384,1024]{1,0:T(8,128)(2,1)S(1)}, bf16[384,1024]{1,0:T(8,128)(2,1)}, u32[]{:S(2)}) copy-start(bf16[384,1024]{1,0:T(8,128)(2,1)} %get-tuple-element.38.refs_0_) | copy-start | bytes 2359300
  21.9 17.0 %copy-start.6 = (bf16[32,384]{0,1:T(8,128)(2,1)}, bf16[32,384]{0,1:T(8,128)(2,1)S(1)}, u32[]{:S(2)}) copy-start(bf16[32,384]{0,1:T(8,128)(2,1)S(1)} %copy.27) | copy-start | bytes 73732
  25.8 26.4 %copy-start.1 = (bf16[384,1024]{1,0:T(8,128)(2,1)}, bf16[384,1024]{1,0:T(8,128)(2,1)S(1)}, u32[]{:S(2)}) copy-start(bf16[384,1024]{1,0:T(8,128)(2,1)S(1)} %collective-permute-done.1.refs_1_) | copy-start | bytes 2359300
  30.7 20.3 %copy-start.2 = (bf16[384,1024]{1,0:T(8,128)(2,1)}, bf16[384,1024]{1,0:T(8,128)(2,1)S(1)}, u32[]{:S(2)}) copy-start(bf16[384,1024]{1,0:T(8,128)(2,1)S(1)} %collective-permute-done.refs_5_) | copy-start | bytes 2359300
  32.9 18.2 %collective-permute-start.7 = (bf16[192,1024]{1,0:T(8,128)(2,1)}, bf16[192,1024]{1,0:T(8,128)(2,1)S(1)}, u32[]{:S(2)}, u32[]{:S(2)}) collective-permute-start(bf16[192,1024]{1,0:T(8,128)(2,1)} %add_convert_fusion.2), channel_id=1, source_target_pairs={{0,8},{4,12},{8,0},{12,4},{16,24},{20,28},{24,16},{28,20},{1,9},{5... | collective-permute-start | bytes 1179656 | tf_op jit(solution)/shard_map/ppermute | solution.py:512
  32.9 19.3 %collective-permute-start.6 = (bf16[192,1024]{1,0:T(8,128)(2,1)}, bf16[192,1024]{1,0:T(8,128)(2,1)}, u32[]{:S(2)}, u32[]{:S(2)}) collective-permute-start(bf16[192,1024]{1,0:T(8,128)(2,1)} %add_convert_fusion.3), channel_id=1, source_target_pairs={{0,16},{4,20},{8,24},{12,28},{16,0},{20,4},{24,8},{28,12},{1,17},{... | collective-permute-start | bytes 1179656 | tf_op jit(solution)/shard_map/ppermute | solution.py:512
  39.5 8.7 %copy-start = (bf16[384,1024]{1,0:T(8,128)(2,1)S(1)}, bf16[384,1024]{1,0:T(8,128)(2,1)}, u32[]{:S(2)}) copy-start(bf16[384,1024]{1,0:T(8,128)(2,1)} %shard_map.253.refs_0_) | copy-start | bytes 2359300
  48.1 6.6 %copy-start.14 = (bf16[32,192]{0,1:T(8,128)(2,1)S(1)}, bf16[32,192]{0,1:T(8,128)(2,1)}, u32[]{:S(2)}) copy-start(bf16[32,192]{0,1:T(8,128)(2,1)} %add_convert_fusion.8) | copy-start | bytes 36868
  48.1 12.1 %copy-start.7 = (bf16[32,384]{0,1:T(8,128)(2,1)S(1)}, bf16[32,384]{0,1:T(8,128)(2,1)}, u32[]{:S(2)}) copy-start(bf16[32,384]{0,1:T(8,128)(2,1)} %copy-done.6) | copy-start | bytes 73732
  48.2 12.1 %copy-start.13 = (bf16[32,384]{0,1:T(8,128)(2,1)S(1)}, bf16[32,384]{0,1:T(8,128)(2,1)}, u32[]{:S(2)}) copy-start(bf16[32,384]{0,1:T(8,128)(2,1)} %copy-done.12) | copy-start | bytes 73732
  49.4 12.7 %collective-permute-start.4 = (bf16[192,1024]{1,0:T(8,128)(2,1)S(1)}, bf16[192,1024]{1,0:T(8,128)(2,1)S(1)}, u32[]{:S(2)}, u32[]{:S(2)}) collective-permute-start(bf16[192,1024]{1,0:T(8,128)(2,1)S(1)} %add_convert_fusion.1), channel_id=1, source_target_pairs={{0,8},{4,12},{8,0},{12,4},{16,24},{20,28},{24,16},{28,20},{1,9},{5... | collective-permute-start | bytes 1179656 | tf_op jit(solution)/shard_map/ppermute | solution.py:512
  51.0 30.5 %copy-start.4 = (bf16[192,1024]{1,0:T(8,128)(2,1)}, bf16[192,1024]{1,0:T(8,128)(2,1)S(1)}, u32[]{:S(2)}) copy-start(bf16[192,1024]{1,0:T(8,128)(2,1)S(1)} %collective-permute-done.7.refs_6_) | copy-start | bytes 1179652
  53.2 45.2 %collective-permute-start.13 = (bf16[1024,512]{1,0:T(8,128)(2,1)}, bf16[1024,512]{1,0:T(8,128)(2,1)S(1)}, u32[]{:S(2)}, u32[]{:S(2)}) collective-permute-start(bf16[1024,512]{1,0:T(8,128)(2,1)} %param.49), channel_id=1, source_target_pairs={{0,4},{4,0},{8,12},{12,8},{16,20},{20,16},{24,28},{28,24},{1,5},{5... | collective-permute-start | bytes 3145736 | tf_op jit(solution)/shard_map/ppermute | solution.py:512
  54.8 5.5 %collective-permute-start.5 = (bf16[32,192]{0,1:T(8,128)(2,1)S(1)}, bf16[32,192]{0,1:T(8,128)(2,1)S(1)}, u32[]{:S(2)}, u32[]{:S(2)}) collective-permute-start(bf16[32,192]{0,1:T(8,128)(2,1)S(1)} %copy-done.14), channel_id=1, source_target_pairs={{0,16},{4,20},{8,24},{12,28},{16,0},{20,4},{24,8},{28,12},{1,17},{... | collective-permute-start | bytes 36872 | tf_op jit(solution)/shard_map/ppermute | solution.py:512
  55.1 26.4 %collective-permute-start.10 = (bf16[96,1024]{1,0:T(8,128)(2,1)S(1)}, bf16[96,1024]{1,0:T(8,128)(2,1)S(1)}, u32[]{:S(2)}, u32[]{:S(2)}) collective-permute-start(bf16[96,1024]{1,0:T(8,128)(2,1)S(1)} %add_convert_fusion.7), channel_id=1, source_target_pairs={{0,16},{4,20},{8,24},{12,28},{16,0},{20,4},{24,8},{28,12},{1,17},{... | collective-permute-start | bytes 589832 | tf_op jit(solution)/shard_map/ppermute | solution.py:512
  57.7 23.8 %collective-permute-start.9 = (bf16[96,1024]{1,0:T(8,128)(2,1)S(1)}, bf16[96,1024]{1,0:T(8,128)(2,1)S(1)}, u32[]{:S(2)}, u32[]{:S(2)}) collective-permute-start(bf16[96,1024]{1,0:T(8,128)(2,1)S(1)} %add_convert_fusion.6), channel_id=1, source_target_pairs={{0,4},{4,0},{8,12},{12,8},{16,20},{20,16},{24,28},{28,24},{1,5},{5... | collective-permute-start | bytes 589832 | tf_op jit(solution)/shard_map/ppermute | solution.py:512
  60.3 20.6 %collective-permute-start.11 = (bf16[32,96]{0,1:T(8,128)(2,1)S(1)}, bf16[32,96]{0,1:T(8,128)(2,1)S(1)}, u32[]{:S(2)}, u32[]{:S(2)}) collective-permute-start(bf16[32,96]{0,1:T(8,128)(2,1)S(1)} %add_convert_fusion.9), channel_id=1, source_target_pairs={{0,4},{4,0},{8,12},{12,8},{16,20},{20,16},{24,28},{28,24},{1,5},{5... | collective-permute-start | bytes 18440 | tf_op jit(solution)/shard_map/ppermute | solution.py:512
  62.1 1.2 copy-start.5
  63.3 24.0 %collective-permute-start.8 = (bf16[96,1024]{1,0:T(8,128)(2,1)S(1)}, bf16[96,1024]{1,0:T(8,128)(2,1)S(1)}, u32[]{:S(2)}, u32[]{:S(2)}) collective-permute-start(bf16[96,1024]{1,0:T(8,128)(2,1)S(1)} %add_convert_fusion.5), channel_id=1, source_target_pairs={{0,16},{4,20},{8,24},{12,28},{16,0},{20,4},{24,8},{28,12},{1,17},{... | collective-permute-start | bytes 589832 | tf_op jit(solution)/shard_map/ppermute | solution.py:512
  90.3 8.1 %collective-permute-start.14 = (bf16[96,1024]{1,0:T(8,128)(2,1)}, bf16[96,1024]{1,0:T(8,128)(2,1)S(1)}, u32[]{:S(2)}, u32[]{:S(2)}) collective-permute-start(bf16[96,1024]{1,0:T(8,128)(2,1)} %gate.1), channel_id=1, source_target_pairs={{0,16},{4,20},{8,24},{12,28},{16,0},{20,4},{24,8},{28,12},{1,17},{... | collective-permute-start | bytes 589832 | tf_op jit(solution)/shard_map/ppermute | solution.py:512
  90.6 9.1 %copy-start.8 = (bf16[96,1024]{1,0:T(8,128)(2,1)S(1)}, bf16[96,1024]{1,0:T(8,128)(2,1)}, u32[]{:S(2)}) copy-start(bf16[96,1024]{1,0:T(8,128)(2,1)} %gate.1) | copy-start | bytes 589828
  90.6 9.6 %collective-permute-start.12 = (bf16[96,1024]{1,0:T(8,128)(2,1)}, bf16[96,1024]{1,0:T(8,128)(2,1)S(1)}, u32[]{:S(2)}, u32[]{:S(2)}) collective-permute-start(bf16[96,1024]{1,0:T(8,128)(2,1)} %gate.1), channel_id=1, source_target_pairs={{0,8},{4,12},{8,0},{12,4},{16,24},{20,28},{24,16},{28,20},{1,9},{5... | collective-permute-start | bytes 589832 | tf_op jit(solution)/shard_map/ppermute | solution.py:512
  98.4 5.7 %collective-permute-start.15 = (bf16[96,1024]{1,0:T(8,128)(2,1)S(1)}, bf16[96,1024]{1,0:T(8,128)(2,1)S(1)}, u32[]{:S(2)}, u32[]{:S(2)}) collective-permute-start(bf16[96,1024]{1,0:T(8,128)(2,1)S(1)} %collective-permute-done.14), channel_id=1, source_target_pairs={{0,8},{4,12},{8,0},{12,4},{16,24},{20,28},{24,16},{28,20},{1,9},{5... | collective-permute-start | bytes 589832 | tf_op jit(solution)/shard_map/ppermute | solution.py:512
  104.5 1.8 %collective-permute-start.16 = (bf16[192,1024]{1,0:T(8,128)(2,1)S(1)}, bf16[192,1024]{1,0:T(8,128)(2,1)S(1)}, u32[]{:S(2)}, u32[]{:S(2)}) collective-permute-start(bf16[192,1024]{1,0:T(8,128)(2,1)S(1)} %pad_maximum_fusion.1), channel_id=1, source_target_pairs={{0,1},{1,0},{2,3},{3,2},{4,5},{5,4},{6,7},{7,6},{8,9},{9,8},{10,11... | collective-permute-start | bytes 1179656 | tf_op jit(solution)/shard_map/ppermute | solution.py:678
  106.5 6.1 %collective-permute-start.17 = (bf16[96,1024]{1,0:T(8,128)(2,1)S(1)}, bf16[96,1024]{1,0:T(8,128)(2,1)S(1)}, u32[]{:S(2)}, u32[]{:S(2)}) collective-permute-start(bf16[96,1024]{1,0:T(8,128)(2,1)S(1)} %get-tuple-element.68), channel_id=1, source_target_pairs={{0,0},{1,8},{2,16},{3,24},{4,4},{5,12},{6,20},{7,28},{8,1},{9,9},{... | collective-permute-start | bytes 589832 | tf_op jit(solution)/shard_map/ppermute | solution.py:697
  107.2 10.7 %collective-permute-start.18 = (bf16[96,1024]{1,0:T(8,128)(2,1)S(1)}, bf16[96,1024]{1,0:T(8,128)(2,1)S(1)}, u32[]{:S(2)}, u32[]{:S(2)}) collective-permute-start(bf16[96,1024]{1,0:T(8,128)(2,1)S(1)} %get-tuple-element.69), channel_id=1, source_target_pairs={{0,16},{1,24},{2,0},{3,8},{4,20},{5,28},{6,4},{7,12},{8,17},{9,25}... | collective-permute-start | bytes 589832 | tf_op jit(solution)/shard_map/ppermute | solution.py:697
  (4 other events, 2.8 us)
